TPU v7x, 512 devices: a whole 4x8x8 slice. The times are simulated.
512 devices in a mesh: ep: 128 (over z, y, core), tp: 4 (over x).
Axes of the slice: x: 4, y: 8, z: 8, core: 2. Of those that a mesh axis runs over, the one named last changes fastest.
Arguments:
- tokens: bfloat16 [1024, 1024], P('ep'), may hold values from -6 to 6
- mix_gain: float32 [1024], replicated, may hold values from 0.1 to 1.9
- w_query: bfloat16 [1024, 512], P(None, 'tp'), may hold values from -0.1875 to 0.1875
- w_key: bfloat16 [1024, 512], P(None, 'tp'), may hold values from -0.1875 to 0.1875
- w_value: bfloat16 [1024, 1024], P(None, 'tp'), may hold values from -0.1875 to 0.1875
- w_ogate: bfloat16 [1024, 1024], P(None, 'tp'), may hold values from -0.1875 to 0.1875
- w_igate: bfloat16 [1024, 4], replicated, may hold values from -0.1875 to 0.1875
- w_fgate: bfloat16 [1024, 4], replicated, may hold values from -0.1875 to 0.1875
- forget_bias: float32 [4], replicated, may hold values from -1 to 3
- head_gain: float32 [1024], P('tp'), may hold values from 0.1 to 1.9
- w_out: bfloat16 [1024, 1024], P('tp'), may hold values from -0.1875 to 0.1875
- memory: float32 [1024, 4, 128, 256], P('ep', 'tp'), may hold values from -0.4 to 0.4
- normalizer: float32 [1024, 4, 128], P('ep', 'tp'), may hold values from -0.4 to 0.4
- running_max: float32 [1024, 4], P('ep', 'tp'), may hold values from -4 to 4
- ffn_gain: float32 [1024], replicated, may hold values from 0.1 to 1.9
- route: int32 [1024, 2], replicated, may hold values from 0 to 127, all different within a row; in each aligned block of 1024 rows (0 to 1023, 1024 to 2047, ...) at most 32 rows name the same one
- route_weight: float32 [1024, 2], replicated, may hold values from 0.05 to 1
- w_gate: bfloat16 [128, 1024, 512], P('ep', None, 'tp'), may hold values from -0.1875 to 0.1875
- w_up: bfloat16 [128, 1024, 512], P('ep', None, 'tp'), may hold values from -0.1875 to 0.1875
- w_down: bfloat16 [128, 512, 1024], P('ep', 'tp'), may hold values from -0.25 to 0.25
Outputs:
- mixed: bfloat16 [1024, 1024], P(None, 'ep')
- new_memory: float32 [1024, 4, 128, 256], P('ep', 'tp')
- new_normalizer: float32 [1024, 4, 128], P('ep', 'tp')
- new_max: float32 [1024, 4], P('ep', 'tp')
Inputs may be any that keep to these rules, and one draw needn't show every extreme that they name: `route`: each expert is named by at most 32 routes in all, a bound that some block reaches; the two choices of a token differ.
All inputs are finite; a program needn't handle non-finite values.
Results may differ from a plain program's by a relative error of at most 0.014.
Values may be sent and summed in bfloat16 or wider, within the bound.
A program may use at most 64 MiB of HBM per device.

v0:
```python
import jax
import jax.numpy as jnp
from jax import lax
from jax.sharding import Mesh
from jax.sharding import PartitionSpec as P

EXPERT_CAPACITY = 32
EP = ("ep_0", "ep_1", "ep_2")


EPS = 1e-06


def from_everyone(array, axis):
    length = lax.axis_size(axis)
    return lax.all_to_all(
        jnp.broadcast_to(array[None], (length, *array.shape)), axis, 0, 0, tiled=True
    )


def over_copies(array, axis):
    return from_everyone(array, axis).astype(jnp.float32).sum(axis=0)


def split_up(array, dim, length):
    dims = array.shape
    pieces = array.reshape(*dims[:dim], length, dims[dim] // length, *dims[dim + 1 :])
    return jnp.moveaxis(pieces, dim, 0)


def joined_along(pieces, dim):
    dims = list(pieces.shape[1:])
    dims[dim] *= pieces.shape[0]
    return jnp.moveaxis(pieces, 0, dim).reshape(dims)


def exchange_in_order(pieces, axes, order):
    dims = [lax.axis_size(a) for a in axes]
    pieces = pieces.reshape(*dims, *pieces.shape[1:])
    for k in order:
        pieces = lax.all_to_all(pieces, axes[k], split_axis=k, concat_axis=k, tiled=True)
    return pieces.reshape(-1, *pieces.shape[len(axes) :])


def core_and_chips(array, groups, order, split_dim, concat_dim):
    length = lax.axis_size(groups[0]) * lax.axis_size(groups[1])
    pieces = split_up(array, split_dim, length)
    return joined_along(exchange_in_order(pieces, groups, order), concat_dim)


def round_trip(values):
    rounded = lax.optimization_barrier(values.astype(jnp.bfloat16))
    return rounded.astype(jnp.float32)


def norm_rows(values, gain):
    floats = values.astype(jnp.float32)
    scale = lax.rsqrt(jnp.mean(floats * floats, axis=-1, keepdims=True) + EPS)
    return (floats * scale * gain).astype(jnp.bfloat16)


def slot_targets(route, expert_count, capacity):
    flat = route.reshape(-1)
    onehot = (flat[:, None] == jnp.arange(expert_count, dtype=jnp.int32)[None, :]).astype(jnp.int32)
    before = jnp.cumsum(onehot, axis=0) - onehot
    slot = jnp.sum(before * onehot, axis=1)
    return flat * capacity + slot


def shards(
    tokens,
    mix_gain,
    w_query,
    w_key,
    w_value,
    w_ogate,
    w_igate,
    w_fgate,
    forget_bias,
    head_gain,
    w_out,
    memory,
    normalizer,
    running_max,
    ffn_gain,
    route,
    route_weight,
    w_gate,
    w_up,
    w_down,
):
    width = tokens.shape[1]
    col_count = width // lax.axis_size(EP)
    qk_dim = w_query.shape[1]
    normed = norm_rows(tokens, mix_gain)
    query = round_trip(jnp.dot(normed, w_query, preferred_element_type=jnp.float32))
    scaled_key = round_trip(
        jnp.dot(normed, w_key, preferred_element_type=jnp.float32)
    ) * qk_dim ** (-0.5)
    value = round_trip(jnp.dot(normed, w_value, preferred_element_type=jnp.float32))
    ogate = round_trip(jnp.dot(normed, w_ogate, preferred_element_type=jnp.float32))
    head_pick = (jnp.arange(w_igate.shape[1], dtype=jnp.int32) == lax.axis_index("tp")).astype(
        jnp.float32
    )
    log_in = jnp.sum(
        jnp.dot(normed, w_igate, preferred_element_type=jnp.float32) * head_pick, axis=1
    )
    forget_pre = jnp.sum(
        jnp.dot(normed, w_fgate, preferred_element_type=jnp.float32) * head_pick, axis=1
    )
    log_forget = jax.nn.log_sigmoid(forget_pre + jnp.sum(forget_bias * head_pick))
    old_max = running_max[:, 0]
    new_max = jnp.maximum(log_forget + old_max, log_in)
    keep = jnp.exp(log_forget + old_max - new_max)
    admit = jnp.exp(log_in - new_max)
    state = (
        keep[:, None, None] * memory[:, 0]
        + admit[:, None, None] * scaled_key[:, :, None] * value[:, None, :]
    )
    norm_state = keep[:, None] * normalizer[:, 0] + admit[:, None] * scaled_key
    numer = jnp.einsum("tk,tkv->tv", query, state)
    denom = jnp.sum(query * norm_state, axis=1)
    read = numer / jnp.maximum(jnp.abs(denom), jnp.exp(-new_max))[:, None]
    scale = lax.rsqrt(jnp.mean(read * read, axis=-1, keepdims=True) + EPS)
    gated = (jax.nn.sigmoid(ogate) * read * scale * head_gain).astype(jnp.bfloat16)
    local_output = over_copies(
        jnp.dot(gated, w_out, preferred_element_type=jnp.float32).astype(jnp.bfloat16), "tp"
    ).astype(jnp.float32)
    middle_rows = (tokens.astype(jnp.float32) + local_output).astype(jnp.bfloat16)
    middle = lax.all_to_all(middle_rows, EP, split_axis=1, concat_axis=0, tiled=True)
    expert_count = w_gate.shape[0] * lax.axis_size(EP)
    topk_count = route.shape[1]
    targets = slot_targets(route, expert_count, EXPERT_CAPACITY)
    buffer = (
        jnp.zeros((expert_count * EXPERT_CAPACITY, col_count), jnp.bfloat16)
        .at[targets]
        .set(jnp.repeat(middle, topk_count, axis=0))
    )
    buffer = buffer.reshape(expert_count, EXPERT_CAPACITY, col_count)
    rows = lax.all_to_all(buffer, EP, split_axis=0, concat_axis=2, tiled=True)
    rows = norm_rows(rows, ffn_gain)
    gate_v = jnp.einsum("ecd,edf->ecf", rows, w_gate, preferred_element_type=jnp.float32)
    up_v = jnp.einsum("ecd,edf->ecf", rows, w_up, preferred_element_type=jnp.float32)
    activation = (jax.nn.silu(gate_v) * up_v).astype(jnp.bfloat16)
    partial_value = jnp.einsum(
        "ecf,efd->ecd", activation, w_down, preferred_element_type=jnp.float32
    )
    results = (
        over_copies(partial_value.astype(jnp.bfloat16), "tp")
        .astype(jnp.float32)
        .astype(jnp.bfloat16)
    )
    returned = core_and_chips(results, (("ep_0", "ep_1"), "ep_2"), (1, 0), 2, 0)
    picked = returned.reshape(expert_count * EXPERT_CAPACITY, col_count)[targets]
    picked = picked.reshape(route.shape[0], topk_count, col_count).astype(jnp.float32)
    weights = route_weight / jnp.sum(route_weight, axis=1, keepdims=True)
    mixed = (middle.astype(jnp.float32) + jnp.sum(picked * weights[:, :, None], axis=1)).astype(
        jnp.bfloat16
    )
    return (mixed, state[:, None], norm_state[:, None], new_max[:, None])


def solution(mesh):
    finer = Mesh(mesh.devices.reshape(8, 8, 2, mesh.shape["tp"]), ("ep_0", "ep_1", "ep_2", "tp"))
    in_specs = (
        P(EP, None),
        P(),
        P(None, "tp"),
        P(None, "tp"),
        P(None, "tp"),
        P(None, "tp"),
        P(),
        P(),
        P(),
        P("tp"),
        P("tp", None),
        P(EP, "tp", None, None),
        P(EP, "tp", None),
        P(EP, "tp"),
        P(),
        P(),
        P(),
        P(EP, None, "tp"),
        P(EP, None, "tp"),
        P(EP, "tp", None),
    )
    out_specs = (P(None, EP), P(EP, "tp", None, None), P(EP, "tp", None), P(EP, "tp"))
    return jax.shard_map(
        shards, mesh=finer, in_specs=in_specs, out_specs=out_specs, check_vma=False
    )
```

profile of v0, /device:TPU:1, one launch (start us, length us, event | category | flops | bytes accessed | tf_op | source)
XLA Modules:
  0.0 134.3 jit_solution(17217719910354161539)
XLA Ops:
  0.7 1.0 fusion.30
  1.6 0.9 fusion.2
  2.6 0.9 fusion.1
  3.5 1.3 fusion.47
  4.8 1.3 exponential_bitcast_fusion
  6.1 1.3 fusion.45
  7.4 1.3 convolution_convert_fusion.3
  8.7 1.2 convolution_convert_fusion.5
  9.9 1.1 convolution_convert_fusion.4
  11.1 0.7 copy-done.7
  11.7 0.8 multiply_reduce_fusion.1
  12.5 1.2 convolution_convert_fusion.2
  13.8 0.3 fusion.7
  14.1 0.2 multiply_reduce_fusion
  14.4 0.7 copy-done.11
  15.0 0.2 convolution_convert_fusion.1
  15.2 0.7 broadcast_in_dim.10
  15.9 5.0 %all-to-all-start = ((bf16[4,8,1024]{2,1,0:T(8,128)(2,1)}), bf16[4,8,1024]{2,1,0:T(8,128)(2,1)S(1)}, u32[]{:S(2)}, u32[]{:S(2)}) async-start(bf16[4,8,1024]{2,1,0:T(8,128)(2,1)} %broadcast_in_dim.10), calls=%async_computation | async-start | bytes 131072 | tf_op jit(solution)/shard_map/all_to_all | solution.py:16
  20.9 0.2 copy.83
  21.1 0.3 eq.41
  21.4 0.3 eq.37
  21.6 0.1 copy.85
  21.7 0.3 fusion.9
  22.2 0.3 copy.86
  22.5 0.6 fusion.5
  23.2 0.2 copy.82
  23.4 0.3 mul.253
  23.7 1.6 %all-to-all-done = bf16[4,8,1024]{2,1,0:T(8,128)(2,1)S(1)} async-done(((bf16[4,8,1024]{2,1,0:T(8,128)(2,1)}), bf16[4,8,1024]{2,1,0:T(8,128)(2,1)S(1)}, u32[]{:S(2)}, u32[]{:S(2)}) %all-to-all-start) | async-done | bytes 65568 | tf_op jit(solution)/shard_map/all_to_all | solution.py:16
  25.4 0.3 all_to_all.34
  25.7 0.9 copy.79
  26.6 19.0 %all-to-all-start.1 = ((bf16[8,128,8]{2,0,1:T(8,128)(2,1)}), bf16[8,128,8]{2,0,1:T(8,128)(2,1)S(1)}, u32[]{:S(2)}, u32[]{:S(2)}) async-start(bf16[8,128,8]{2,0,1:T(8,128)(2,1)} %copy.79), calls=%async_computation.1 | async-start | bytes 524288 | tf_op jit(solution)/shard_map/all_to_all | solution.py:130
  45.6 0.7 copy-done.6
  46.4 0.6 copy-done.4
  47.0 13.8 %all-to-all-done.1 = bf16[8,128,8]{2,0,1:T(8,128)(2,1)S(1)} async-done(((bf16[8,128,8]{2,0,1:T(8,128)(2,1)}), bf16[8,128,8]{2,0,1:T(8,128)(2,1)S(1)}, u32[]{:S(2)}, u32[]{:S(2)}) %all-to-all-start.1) | async-done | bytes 16416 | tf_op jit(solution)/shard_map/all_to_all | solution.py:130
  60.8 0.3 broadcast_in_dim.12
  61.1 6.1 %scatter_custom_fusion = bf16[4096,8]{1,0:T(8,128)(2,1)S(1)} fusion(s32[2048]{0:T(1024)S(1)} %bitcast.143, bf16[2048,8]{1,0:T(8,128)(2,1)S(1)} %bitcast.141, bf16[]{:T(256)} %constant.37.clone.1), kind=kCustom, calls=%fused_computation.36 | custom fusion | bytes 65538 | tf_op jit(solution)/shard_map/scatter | solution.py:137
  67.2 0.4 copy.89
  67.6 0.8 reshape.330
  68.4 5.5 %all-to-all-start.2 = ((bf16[128,2,128]{2,1,0:T(2,128)(2,1)}), bf16[128,2,128]{2,1,0:T(2,128)(2,1)S(1)}, u32[]{:S(2)}, u32[]{:S(2)}) async-start(bf16[128,2,128]{2,1,0:T(2,128)(2,1)} %reshape.330), calls=%async_computation.2 | async-start | bytes 131072 | tf_op jit(solution)/shard_map/all_to_all | solution.py:140
  73.9 0.2 copy.94
  74.2 11.3 %all-to-all-done.2 = bf16[128,2,128]{2,1,0:T(2,128)(2,1)S(1)} async-done(((bf16[128,2,128]{2,1,0:T(2,128)(2,1)}), bf16[128,2,128]{2,1,0:T(2,128)(2,1)S(1)}, u32[]{:S(2)}, u32[]{:S(2)}) %all-to-all-start.2) | async-done | bytes 65568 | tf_op jit(solution)/shard_map/all_to_all | solution.py:140
  85.4 0.2 reshape.331
  85.6 0.2 fusion.12
  85.8 0.4 fusion.25
  86.2 0.6 copy-done.10
  86.7 1.4 %convolution_convert_fusion = bf16[32,1024]{1,0:T(8,128)(2,1)S(1)} fusion(bf16[1,128,1024]{2,1,0:T(8,128)(2,1)S(1)} %copy-done.10, bf16[1,1024,128]{2,1,0:T(8,128)(2,1)} %param.38, f32[128,8]{1,0:T(8,128)S(1)} %mul.258, f32[32]{0:T(128)S(1)} %add_rsqrt_fusion, f32[32,128]{1,0:T(8,128)S(1)} %fusion.25, bf16[128,8,32]{2,1,0:T(8,128)(2,1)S(1)} %reshape.331), kind=kOutput, calls=%fused_computation.2 | convolution fusion | flops 16965632 | bytes 675968 | tf_op jit(solution)/shard_map/ecf,efd->ecd/dot_general | solution.py:145
  88.2 0.7 broadcast_in_dim.13
  88.9 3.6 %all-to-all-start.3 = ((bf16[4,1,32,1024]{3,2,1,0:T(8,128)(2,1)}), bf16[4,1,32,1024]{3,2,1,0:T(8,128)(2,1)S(1)}, u32[]{:S(2)}, u32[]{:S(2)}) async-start(bf16[4,1,32,1024]{3,2,1,0:T(8,128)(2,1)} %broadcast_in_dim.13), calls=%async_computation.3 | async-start | bytes 524288 | tf_op jit(solution)/shard_map/all_to_all | solution.py:16
  92.5 1.2 multiply_add_fusion
  93.7 4.5 %all-to-all-done.3 = bf16[4,1,32,1024]{3,2,1,0:T(8,128)(2,1)S(1)} async-done(((bf16[4,1,32,1024]{3,2,1,0:T(8,128)(2,1)}), bf16[4,1,32,1024]{3,2,1,0:T(8,128)(2,1)S(1)}, u32[]{:S(2)}, u32[]{:S(2)}) %all-to-all-start.3) | async-done | bytes 262176 | tf_op jit(solution)/shard_map/all_to_all | solution.py:16
  98.2 0.2 copy.90
  98.4 0.3 copy.91
  98.7 0.2 reshape.332
  98.9 5.2 %all_to_all.48 = bf16[2,2,8192]{2,1,0:T(2,128)(2,1)S(1)} all-to-all(bf16[2,2,8192]{2,1,0:T(2,128)(2,1)S(1)} %reshape.332), channel_id=1, replica_groups=mesh['ep_0'=8,'ep_1'=8,'ep_2'=2,'tp'=4] {'ep_2'}, dimensions={0} | all-to-all | bytes 131072 | tf_op jit(solution)/shard_map/all_to_all | solution.py:41
  104.0 0.1 reshape.333
  104.2 0.3 copy.92
  104.5 0.8 reshape.334
  105.3 4.6 %all-to-all-start.5 = ((bf16[64,2,256]{2,1,0:T(2,128)(2,1)}), bf16[64,2,256]{2,1,0:T(2,128)(2,1)S(1)}, u32[]{:S(2)}, u32[]{:S(2)}) async-start(bf16[64,2,256]{2,1,0:T(2,128)(2,1)} %reshape.334), calls=%async_computation.5 | async-start | bytes 131072 | tf_op jit(solution)/shard_map/all_to_all | solution.py:41
  109.9 11.1 %all-to-all-done.5 = bf16[64,2,256]{2,1,0:T(2,128)(2,1)S(1)} async-done(((bf16[64,2,256]{2,1,0:T(2,128)(2,1)}), bf16[64,2,256]{2,1,0:T(2,128)(2,1)S(1)}, u32[]{:S(2)}, u32[]{:S(2)}) %all-to-all-start.5) | async-done | bytes 65568 | tf_op jit(solution)/shard_map/all_to_all | solution.py:41
  121.0 0.2 reshape.335
  121.2 0.5 copy.93
  121.6 6.2 %gather_fusion = bf16[2048,8]{1,0:T(8,128)(2,1)S(1)} fusion(bf16[4096,8]{1,0:T(8,128)(2,1)S(1)} %bitcast.131, s32[2048]{0:T(1024)S(1)} %broadcast_clamp_fusion), kind=kCustom, calls=%fused_computation | custom fusion | bytes 73728 | tf_op jit(solution)/shard_map/gather | solution.py:154
  127.8 5.6 %fusion.3 = f32[1024,8]{1,0:T(8,128)S(1)} fusion(bf16[1024,2,8]{2,1,0:T(2,128)(2,1)S(1)} %bitcast.134, f32[1024,2]{1,0:T(8,128)S(1)} %copy.94), kind=kLoop, calls=%fused_computation.15 | loop fusion | flops 40960 | bytes 73728 | tf_op jit(solution)/shard_map/reduce_sum | solution.py:157
  133.5 0.7 copy.95
  (41 shorter events, 0.5 us)
Async XLA Ops:
  0.6 13.7 %copy-start = (bf16[256,1024]{1,0:T(8,128)(2,1)S(1)}, bf16[256,1024]{1,0:T(8,128)(2,1)}, u32[]{:S(2)}) copy-start(bf16[256,1024]{1,0:T(8,128)(2,1)} %param.30) | copy-start | bytes 1572868
  0.6 1.0 copy-start.2
  0.7 13.1 %copy-start.1 = (f32[8,1,128,256]{3,2,1,0:T(8,128)S(1)}, f32[8,1,128,256]{3,2,1,0:T(8,128)}, u32[]{:S(2)}) copy-start(f32[8,1,128,256]{3,2,1,0:T(8,128)} %param.31) | copy-start | bytes 3145732
  6.1 6.5 %copy-start.8 = (f32[8,1]{0,1:T(1,128)}, f32[8,1]{0,1:T(1,128)S(1)}, u32[]{:S(2)}) copy-start(f32[8,1]{0,1:T(1,128)S(1)} %get-tuple-element.33) | copy-start | bytes 100
  8.7 1.2 copy-start.5
  11.0 0.7 copy-start.7
  14.3 0.7 copy-start.11
  15.9 5.0 %copy-start.3 = (s32[1024,2]{0,1:T(2,128)S(1)}, s32[1024,2]{0,1:T(2,128)}, u32[]{:S(2)}) copy-start(s32[1024,2]{0,1:T(2,128)} %param.35) | copy-start | bytes 24580
  15.9 9.4 %all-to-all-start = ((bf16[4,8,1024]{2,1,0:T(8,128)(2,1)}), bf16[4,8,1024]{2,1,0:T(8,128)(2,1)S(1)}, u32[]{:S(2)}, u32[]{:S(2)}) async-start(bf16[4,8,1024]{2,1,0:T(8,128)(2,1)} %broadcast_in_dim.10), calls=%async_computation | async-start | bytes 131072 | tf_op jit(solution)/shard_map/all_to_all | solution.py:16
  26.6 34.3 %all-to-all-start.1 = ((bf16[8,128,8]{2,0,1:T(8,128)(2,1)}), bf16[8,128,8]{2,0,1:T(8,128)(2,1)S(1)}, u32[]{:S(2)}, u32[]{:S(2)}) async-start(bf16[8,128,8]{2,0,1:T(8,128)(2,1)} %copy.79), calls=%async_computation.1 | async-start | bytes 524288 | tf_op jit(solution)/shard_map/all_to_all | solution.py:130
  45.6 0.7 copy-start.6
  46.3 0.7 copy-start.4
  68.4 17.1 %all-to-all-start.2 = ((bf16[128,2,128]{2,1,0:T(2,128)(2,1)}), bf16[128,2,128]{2,1,0:T(2,128)(2,1)S(1)}, u32[]{:S(2)}, u32[]{:S(2)}) async-start(bf16[128,2,128]{2,1,0:T(2,128)(2,1)} %reshape.330), calls=%async_computation.2 | async-start | bytes 131072 | tf_op jit(solution)/shard_map/all_to_all | solution.py:140
  74.2 11.6 %copy-start.9 = (bf16[1,1024,128]{2,1,0:T(8,128)(2,1)S(1)}, bf16[1,1024,128]{2,1,0:T(8,128)(2,1)}, u32[]{:S(2)}) copy-start(bf16[1,1024,128]{2,1,0:T(8,128)(2,1)} %param.37) | copy-start | bytes 786436
  85.8 1.0 copy-start.10
  88.9 9.3 %all-to-all-start.3 = ((bf16[4,1,32,1024]{3,2,1,0:T(8,128)(2,1)}), bf16[4,1,32,1024]{3,2,1,0:T(8,128)(2,1)S(1)}, u32[]{:S(2)}, u32[]{:S(2)}) async-start(bf16[4,1,32,1024]{3,2,1,0:T(8,128)(2,1)} %broadcast_in_dim.13), calls=%async_computation.3 | async-start | bytes 524288 | tf_op jit(solution)/shard_map/all_to_all | solution.py:16
  105.3 15.7 %all-to-all-start.5 = ((bf16[64,2,256]{2,1,0:T(2,128)(2,1)}), bf16[64,2,256]{2,1,0:T(2,128)(2,1)S(1)}, u32[]{:S(2)}, u32[]{:S(2)}) async-start(bf16[64,2,256]{2,1,0:T(2,128)(2,1)} %reshape.334), calls=%async_computation.5 | async-start | bytes 131072 | tf_op jit(solution)/shard_map/all_to_all | solution.py:41
where the time goes:
time: 135 us; the launch traced here: 134 us
  waiting for transfers between devices  42.3 us (31%)
  starting transfers between devices  37.7 us (28%)
  local copies, waits for them, and re-layouts  25 us (19%)
  other arithmetic  14.1 us (10%)
  matrix products  9.06 us (7%)
  blocking collectives  5.16 us (4%)
    all_to_all x1, starting transfers between devices, shards(): lax.all_to_all(middle_rows, EP, split_axis=1, concat_axis=0, tiled=True)  19 us
    all_to_all x1, waiting for transfers between devices, shards(): lax.all_to_all(middle_rows, EP, split_axis=1, concat_axis=0, tiled=True)  13.8 us
    all_to_all x1, waiting for transfers between devices, shards(): rows = lax.all_to_all(buffer, EP, split_axis=0, concat_axis=2, tiled=True)  11.3 us
    all_to_all x1, waiting for transfers between devices, exchange_in_order(): lax.all_to_all(pieces, axes[k], split_axis=k, concat_axis=k, tiled=True)  11.1 us
    all_to_all x2, starting transfers between devices, from_everyone(): lax.all_to_all(jnp.broadcast_to(array[None], (length, *array.shape)), axi...  8.55 us
    unnamed x32, local copies, waits for them, and re-layouts  6.42 us
    gather x1, local copies, waits for them, and re-layouts, shards(): returned.reshape(expert_count * EXPERT_CAPACITY, col_count)[targets]  6.18 us
    all_to_all x2, waiting for transfers between devices, from_everyone(): lax.all_to_all(jnp.broadcast_to(array[None], (length, *array.shape)), axi...  6.1 us
  transfers between devices with their start and end apart: 5, of which 5 were waited for; matrix products, arithmetic and copies ran while one was open for 3% of the time, Pallas kernels for 0%

commit v1 on v0

v1 whole, which is shorter than its diff:
```python
import functools

import jax
import jax.numpy as jnp
from jax import lax
from jax.experimental import pallas as pl
from jax.experimental.pallas import tpu as pltpu
from jax.sharding import Mesh
from jax.sharding import PartitionSpec as P

MESH = pl.DeviceIdType.MESH
CAP = 32
LANES = 128
EPS = 1e-06
F32 = jnp.float32
BF16 = jnp.bfloat16


def dot(a, b):
    return jnp.dot(a, b, preferred_element_type=F32)


def kernel(
    sizes,
    tok_h,
    mix_h,
    wq_h,
    wk_h,
    wv_h,
    wo_h,
    wi_h,
    wf_h,
    fb_h,
    hg_h,
    wout_h,
    mem_h,
    nrm_h,
    rmax_h,
    fg_h,
    route_h,
    rw_h,
    wgate_h,
    wup_h,
    wdown_h,
    mixed_ref,
    keep_ref,
    akey_ref,
    value_ref,
    newnorm_ref,
    newmax_ref,
    tok,
    mix,
    wq,
    wk,
    wv,
    wo,
    wi,
    wf,
    fb,
    hg,
    wout,
    mem,
    nrm,
    rmax,
    fg,
    route,
    rw,
    wgate,
    wup,
    wdown,
    load_sem,
    tgt,
    place,
    psend,
    precv,
    csend,
    crecv,
    esend,
    erecv,
    rsend,
    rrecv,
    stage,
    dsend,
    frecv,
    psem,
    csem,
    esem,
    rsem,
    dsem,
):
    nz, ny, nc, nx = sizes
    z, y, c, x = (lax.axis_index(a) for a in ("z", "y", "c", "x"))
    zy = z * ny + y
    ep = zy * nc + c
    rows, width = tok.shape
    groups = nx * nc
    quarter = width // nx
    chips = nz * ny
    owned = width // (chips * nc)
    owners = LANES // owned
    group = x * nc + c
    expert_count = chips * nc
    token_count = route.shape[1]

    hbm = (tok_h, mix_h, wq_h, wk_h, wv_h, wo_h, wi_h, wf_h, fb_h, hg_h, wout_h, mem_h, nrm_h, rmax_h)
    hbm += (fg_h, route_h, rw_h, wgate_h, wup_h, wdown_h)
    vmem = (tok, mix, wq, wk, wv, wo, wi, wf, fb, hg, wout, mem, nrm, rmax)
    vmem += (fg, route, rw, wgate, wup, wdown)
    loads = [pltpu.make_async_copy(h, v, load_sem.at[i]) for i, (h, v) in enumerate(zip(hbm, vmem))]
    for load in loads:
        load.start()

    barrier = pltpu.get_barrier_semaphore()

    def greet(target):
        pl.semaphore_signal(barrier, inc=1, device_id=target, device_id_type=MESH)

    def greet_plane(i, carry):
        tz, ty = lax.rem(z + i // ny, nz), lax.rem(y + i % ny, ny)

        @pl.when(i > 0)
        def _():
            greet((tz, ty, c, x))

        for dc in range(1, nc):
            greet((tz, ty, lax.rem(c + dc, nc), x))
        return carry

    lax.fori_loop(0, chips, greet_plane, 0)
    for dx in range(1, nx):
        for dc in range(nc):
            greet((z, y, lax.rem(c + dc, nc), lax.rem(x + dx, nx)))
    source_group = ep // owners
    source_x, source_c = source_group // nc, source_group % nc
    from_self = source_group == group

    def greet_sources(i, carry):
        tz, ty = lax.rem(z + i // ny, nz), lax.rem(y + i % ny, ny)

        @pl.when(jnp.logical_or(i > 0, jnp.logical_not(from_self)))
        def _():
            greet((tz, ty, source_c, source_x))

        return carry

    lax.fori_loop(0, chips, greet_sources, 0)

    for i in range(14):
        loads[i].wait()
    tokens = tok[...].astype(F32)
    mean = jnp.mean(tokens * tokens, axis=1, keepdims=True)
    normed = (tokens * lax.rsqrt(mean + EPS) * mix[...]).astype(BF16)
    query16 = dot(normed, wq[...]).astype(BF16)
    query = query16.astype(F32)
    qk = wq.shape[1]
    scaled_key = dot(normed, wk[...]).astype(BF16).astype(F32) * qk ** (-0.5)
    value = dot(normed, wv[...]).astype(BF16).astype(F32)
    ogate = dot(normed, wo[...]).astype(BF16).astype(F32)
    floats = normed.astype(F32)
    head_row = lax.broadcasted_iota(jnp.int32, wi.shape, 0) == x
    in_row = jnp.sum(jnp.where(head_row, wi[...].astype(F32), 0.0), axis=0, keepdims=True)
    forget_row = jnp.sum(jnp.where(head_row, wf[...].astype(F32), 0.0), axis=0, keepdims=True)
    log_in = jnp.sum(floats * in_row, axis=1, keepdims=True)
    head_lane = lax.broadcasted_iota(jnp.int32, fb.shape, 1) == x
    bias = jnp.sum(jnp.where(head_lane, fb[...], 0.0), axis=1, keepdims=True)
    forget_pre = jnp.sum(floats * forget_row, axis=1, keepdims=True) + bias
    log_forget = jnp.minimum(forget_pre, 0.0) - jnp.log1p(jnp.exp(-jnp.abs(forget_pre)))
    diagonal = lax.broadcasted_iota(jnp.int32, (rows, rows), 0) == lax.broadcasted_iota(
        jnp.int32, (rows, rows), 1
    )
    old_max = jnp.sum(
        jnp.where(diagonal, jnp.broadcast_to(rmax[...], (rows, rows)), 0.0), axis=1, keepdims=True
    )
    carried = log_forget + old_max
    new_max = jnp.maximum(carried, log_in)
    keep = jnp.exp(carried - new_max)
    admit = jnp.exp(log_in - new_max)
    akey = admit * scaled_key
    norm_state = keep * nrm[...] + akey
    keep_ref[...] = jnp.broadcast_to(keep, keep_ref.shape)
    akey_ref[...] = akey
    value_ref[...] = value
    newnorm_ref[...] = norm_state
    newmax_ref[...] = jnp.sum(
        jnp.where(diagonal, jnp.broadcast_to(new_max, (rows, rows)), 0.0), axis=0, keepdims=True
    )
    row_of = lax.broadcasted_iota(jnp.int32, value.shape, 0)
    kept = jnp.zeros_like(value)
    for t in range(rows):
        kept = jnp.where(row_of == t, dot(query16, mem[t].astype(BF16)), kept)
    numer = keep * kept + jnp.sum(query * akey, axis=1, keepdims=True) * value
    denom = jnp.sum(query * norm_state, axis=1, keepdims=True)
    read = numer / jnp.maximum(jnp.abs(denom), jnp.exp(-new_max))
    scale = lax.rsqrt(jnp.mean(read * read, axis=1, keepdims=True) + EPS)
    gated = (jax.nn.sigmoid(ogate) * read * scale * hg[...]).astype(BF16)
    partial = dot(gated, wout[...]).astype(BF16)
    for i in range(nx):
        psend[i] = partial[:, i * quarter : (i + 1) * quarter]

    loads[15].wait()
    expert_of = lax.broadcasted_iota(jnp.int32, (expert_count, token_count), 0)
    named = [expert_of == route[j : j + 1, :] for j in range(2)]
    either = jnp.where(jnp.logical_or(named[0], named[1]), 1.0, 0.0)
    block = min(256, token_count)
    earlier = (
        lax.broadcasted_iota(jnp.int32, (block, block), 0)
        < lax.broadcasted_iota(jnp.int32, (block, block), 1)
    ).astype(F32).astype(BF16)
    carry = jnp.zeros((expert_count, 1), F32)
    before = []
    for b in range(token_count // block):
        part = either[:, b * block : (b + 1) * block]
        before.append(dot(part.astype(BF16), earlier) + carry)
        carry = carry + jnp.sum(part, axis=1, keepdims=True)
    before = jnp.concatenate(before, axis=1)
    for j in range(2):
        slot = jnp.sum(jnp.where(named[j], before, 0.0), axis=0, keepdims=True)
        tgt[j : j + 1, :] = route[j : j + 1, :] * CAP + slot.astype(jnp.int32)
    slots_here = nc * CAP
    slot_id = lax.broadcasted_iota(jnp.int32, (slots_here, token_count), 0) + zy * slots_here
    hit = jnp.logical_or(slot_id == tgt[0:1, :], slot_id == tgt[1:2, :])
    place[...] = jnp.where(hit, 1.0, 0.0).astype(BF16)

    own_target = jnp.where(from_self, 1, 0)
    pl.semaphore_wait(barrier, chips * nc - 1 + (nx - 1) * nc + owners * nx - own_target)

    for dx in range(1, nx):
        tx = lax.rem(x + dx, nx)
        pltpu.make_async_remote_copy(
            src_ref=psend.at[tx],
            dst_ref=precv.at[dx - 1],
            send_sem=psem.at[0, dx - 1],
            recv_sem=psem.at[1, dx - 1],
            device_id=(z, y, c, tx),
            device_id_type=MESH,
        ).start()
    total = psend[x].astype(F32)
    for dx in range(1, nx):
        copy = pltpu.make_async_remote_copy(
            src_ref=psend.at[0],
            dst_ref=precv.at[dx - 1],
            send_sem=psem.at[0, dx - 1],
            recv_sem=psem.at[1, dx - 1],
            device_id=(z, y, c, lax.rem(x + dx, nx)),
            device_id_type=MESH,
        )
        copy.wait_recv()
        total = total + precv[dx - 1].astype(F32)
    own = tok[:, pl.ds(pl.multiple_of(x * quarter, quarter), quarter)].astype(F32)
    middle = (own + total).astype(BF16)
    for i in range(nc):
        csend[i] = middle[:, i * LANES : (i + 1) * LANES]

    def send_plane(i, carry):
        tz, ty = lax.rem(z + i // ny, nz), lax.rem(y + i % ny, ny)

        def send(tc):
            pltpu.make_async_remote_copy(
                src_ref=csend.at[tc],
                dst_ref=crecv.at[ep],
                send_sem=csem.at[0],
                recv_sem=csem.at[1],
                device_id=(tz, ty, tc, x),
                device_id_type=MESH,
            ).start()

        for dc in range(1, nc):
            send(lax.rem(c + dc, nc))

        @pl.when(i > 0)
        def _():
            send(c)

        return carry

    lax.fori_loop(0, chips, send_plane, 0)
    crecv[ep] = csend[c]
    others = crecv.at[pl.ds(0, chips * nc - 1)]
    plane = pltpu.make_async_remote_copy(
        src_ref=others,
        dst_ref=others,
        send_sem=csem.at[0],
        recv_sem=csem.at[1],
        device_id=(z, y, lax.rem(c + 1, nc), x),
        device_id_type=MESH,
    )
    plane.wait_recv()
    everyone = crecv[...].astype(F32).reshape(token_count, LANES).astype(BF16)
    slots = dot(place[...], everyone).astype(BF16)
    for i in range(nc):
        esend[i] = slots[i * CAP : (i + 1) * CAP]

    def chip_row(send, recv, sem, src_of, dst):
        copies = []
        for dx in range(nx):
            for dc in range(nc):
                if dx == 0 and dc == 0:
                    continue
                tx, tc = lax.rem(x + dx, nx), lax.rem(c + dc, nc)
                n = dx * nc + dc - 1
                copy = pltpu.make_async_remote_copy(
                    src_ref=send.at[src_of(tx, tc)],
                    dst_ref=recv.at[dst],
                    send_sem=sem.at[0, n],
                    recv_sem=sem.at[1, n],
                    device_id=(z, y, tc, tx),
                    device_id_type=MESH,
                )
                copy.start()
                copies.append(copy)
        return copies

    to_experts = chip_row(esend, erecv, esem, lambda tx, tc: tc, group)
    erecv[group] = esend[c]
    for i in (14, 17, 18, 19):
        loads[i].wait()
    for copy in to_experts:
        copy.wait_recv()
    stacked = jnp.concatenate([erecv[i] for i in range(groups)], axis=1).astype(F32)
    mean = jnp.mean(stacked * stacked, axis=1, keepdims=True)
    routed = (stacked * lax.rsqrt(mean + EPS) * fg[...]).astype(BF16)
    gate_v = dot(routed, wgate[...])
    up_v = dot(routed, wup[...])
    act = (gate_v * jax.nn.sigmoid(gate_v) * up_v).astype(BF16)
    down = dot(act, wdown[...]).astype(BF16)
    for i in range(groups):
        rsend[i] = down[:, i * LANES : (i + 1) * LANES]

    to_groups = chip_row(rsend, rrecv, rsem, lambda tx, tc: tx * nc + tc, group)
    rrecv[group] = rsend[group]
    stage[slots_here:, :] = jnp.zeros((LANES - slots_here, LANES), F32)
    here = nc * rows
    spot = pl.multiple_of(slots_here + lax.rem(zy, 4) * here, here)
    stage[pl.ds(spot, here), :] = crecv[pl.ds(zy * nc, nc)].astype(F32).reshape(here, LANES)
    for copy in to_groups:
        copy.wait_recv()
    for i in range(nc):
        result = rrecv[i].astype(F32)
        for j in range(1, nx):
            result = result + rrecv[j * nc + i].astype(F32)
        stage[i * CAP : (i + 1) * CAP, :] = result
    dsend[...] = stage[...].T.reshape(owners, owned, LANES).astype(BF16)

    count = owners * nx

    def send_owner(i, carry):
        n = lax.rem(i + zy, count)
        k, tx = n // nx, n % nx
        target = group * owners + k
        tc = target % nc
        tzy = target // nc

        @pl.when(jnp.logical_not(jnp.logical_and(target == ep, tx == x)))
        def _():
            pltpu.make_async_remote_copy(
                src_ref=dsend.at[k],
                dst_ref=frecv.at[zy],
                send_sem=dsem.at[0],
                recv_sem=dsem.at[1],
                device_id=(tzy // ny, tzy % ny, tc, tx),
                device_id_type=MESH,
            ).start()

        return carry

    lax.fori_loop(0, count, send_owner, 0)

    def arrivals(n):
        part = frecv.at[pl.ds(0, n)]
        return pltpu.make_async_remote_copy(
            src_ref=part,
            dst_ref=part,
            send_sem=dsem.at[0],
            recv_sem=dsem.at[1],
            device_id=(z, y, lax.rem(c + 1, nc), x),
            device_id_type=MESH,
        )

    loads[16].wait()

    @pl.when(from_self)
    def _():
        frecv[zy] = dsend[lax.rem(ep, owners)]
        arrivals(chips - 1).wait_recv()

    @pl.when(jnp.logical_not(from_self))
    def _():
        arrivals(chips).wait_recv()

    vregs = token_count // LANES
    lane = lax.broadcasted_iota(jnp.int32, (owned, LANES), 1)
    low = lane < slots_here
    names = []
    for j in range(2):
        for k in range(vregs):
            t = jnp.broadcast_to(tgt[j : j + 1, k * LANES : (k + 1) * LANES], (owned, LANES))
            names.append((jnp.bitwise_and(t, LANES - 1), lax.shift_right_logical(t, 7)))

    def pick(p, found):
        second = pltpu.roll(frecv[2 * p + 1].astype(F32), slots_here, 1)
        held = jnp.where(low, frecv[2 * p].astype(F32), second)
        return tuple(
            jnp.where(
                part == p,
                jnp.take_along_axis(held, index, axis=1, mode="promise_in_bounds"),
                f,
            )
            for f, (index, part) in zip(found, names)
        )

    nothing = jnp.zeros((owned, LANES), F32)
    found = lax.fori_loop(0, chips // 2, pick, (nothing,) * (2 * vregs))
    for k in range(vregs):
        halves = []
        for h in range(2):
            half = frecv[8 * k + 4 * h].astype(F32)
            for m in range(1, 4):
                half = half + frecv[8 * k + 4 * h + m].astype(F32)
            halves.append(half)
        mid = jnp.where(low, pltpu.roll(halves[0], slots_here, 1), halves[1])
        w0 = rw[0:1, k * LANES : (k + 1) * LANES]
        w1 = rw[1:2, k * LANES : (k + 1) * LANES]
        both = w0 + w1
        mixed = mid + (found[k] * (w0 / both) + found[vregs + k] * (w1 / both))
        mixed_ref[:, k * LANES : (k + 1) * LANES] = mixed.astype(BF16)

    for dx in range(1, nx):
        pltpu.make_async_remote_copy(
            src_ref=psend.at[0],
            dst_ref=precv.at[dx - 1],
            send_sem=psem.at[0, dx - 1],
            recv_sem=psem.at[1, dx - 1],
            device_id=(z, y, c, lax.rem(x + dx, nx)),
            device_id_type=MESH,
        ).wait_send()
    plane.wait_send()
    for copy in to_experts + to_groups:
        copy.wait_send()

    @pl.when(from_self)
    def _():
        arrivals(count - 1).wait_send()

    @pl.when(jnp.logical_not(from_self))
    def _():
        arrivals(count).wait_send()


def shards(
    sizes,
    tokens,
    mix_gain,
    w_query,
    w_key,
    w_value,
    w_ogate,
    w_igate,
    w_fgate,
    forget_bias,
    head_gain,
    w_out,
    memory,
    normalizer,
    running_max,
    ffn_gain,
    route,
    route_weight,
    w_gate,
    w_up,
    w_down,
):
    nz, ny, nc, nx = sizes
    rows, width = tokens.shape
    qk, dv = memory.shape[2:]
    chips = nz * ny
    quarter = width // nx
    groups = nx * nc
    owned = width // (chips * nc)
    owners = LANES // owned
    token_count = route.shape[0]
    operands = (
        tokens,
        mix_gain.reshape(1, -1),
        w_query,
        w_key,
        w_value,
        w_ogate,
        w_igate.T,
        w_fgate.T,
        forget_bias.reshape(1, -1),
        head_gain.reshape(1, -1),
        w_out,
        memory.reshape(rows, qk, dv),
        normalizer.reshape(rows, qk),
        running_max.T,
        ffn_gain.reshape(1, -1),
        route.T,
        route_weight.T,
        w_gate[0],
        w_up[0],
        w_down[0],
    )
    shape = jax.ShapeDtypeStruct
    vmem = pl.BlockSpec(memory_space=pltpu.VMEM)
    mixed, keep, akey, value, new_norm, new_max = pl.pallas_call(
        functools.partial(kernel, sizes),
        out_shape=(
            shape((owned, token_count), BF16),
            shape((rows, LANES), F32),
            shape((rows, qk), F32),
            shape((rows, dv), F32),
            shape((rows, qk), F32),
            shape((1, rows), F32),
        ),
        in_specs=[pl.BlockSpec(memory_space=pl.ANY)] * len(operands),
        out_specs=(vmem,) * 6,
        scratch_shapes=[pltpu.VMEM(a.shape, a.dtype) for a in operands]
        + [
            pltpu.SemaphoreType.DMA((len(operands),)),
            pltpu.VMEM((2, token_count), jnp.int32),
            pltpu.VMEM((nc * CAP, token_count), BF16),
            pltpu.VMEM((nx, rows, quarter), BF16),
            pltpu.VMEM((nx - 1, rows, quarter), BF16),
            pltpu.VMEM((nc, rows, LANES), BF16),
            pltpu.VMEM((chips * nc, rows, LANES), BF16),
            pltpu.VMEM((nc, CAP, LANES), BF16),
            pltpu.VMEM((groups, CAP, LANES), BF16),
            pltpu.VMEM((groups, CAP, LANES), BF16),
            pltpu.VMEM((groups, CAP, LANES), BF16),
            pltpu.VMEM((LANES, LANES), F32),
            pltpu.VMEM((owners, owned, LANES), BF16),
            pltpu.VMEM((max(chips, owners * nx), owned, LANES), BF16),
            pltpu.SemaphoreType.DMA((2, nx - 1)),
            pltpu.SemaphoreType.DMA((2,)),
            pltpu.SemaphoreType.DMA((2, groups - 1)),
            pltpu.SemaphoreType.DMA((2, groups - 1)),
            pltpu.SemaphoreType.DMA((2,)),
        ],
        compiler_params=pltpu.CompilerParams(collective_id=0, has_side_effects=True),
    )(*operands)
    state = keep[:, :1, None] * memory[:, 0] + akey[:, :, None] * value[:, None, :]
    return (mixed.T, state[:, None], new_norm[:, None], new_max.T)


def solution(mesh):
    nx = mesh.shape["tp"]
    nc = 2
    nz = mesh.shape["ep"] // nc
    ny = 1
    while ny * ny < nz:
        ny *= 2
    nz //= ny
    finer = Mesh(mesh.devices.reshape(nz, ny, nc, nx), ("z", "y", "c", "x"))
    ep = ("z", "y", "c")
    in_specs = (
        P(ep, None),
        P(),
        P(None, "x"),
        P(None, "x"),
        P(None, "x"),
        P(None, "x"),
        P(),
        P(),
        P(),
        P("x"),
        P("x", None),
        P(ep, "x", None, None),
        P(ep, "x", None),
        P(ep, "x"),
        P(),
        P(),
        P(),
        P(ep, None, "x"),
        P(ep, None, "x"),
        P(ep, "x", None),
    )
    out_specs = (P(None, ep), P(ep, "x", None, None), P(ep, "x", None), P(ep, "x"))
    return jax.shard_map(
        functools.partial(shards, (nz, ny, nc, nx)),
        mesh=finer,
        in_specs=in_specs,
        out_specs=out_specs,
        check_vma=False,
    )
```

time: 135 us -> 66.5 us (0.49)
  Pallas kernels: 0 us -> 61.9 us
  waiting for transfers between devices: 42.3 us -> 0 us
  starting transfers between devices: 37.7 us -> 0 us
  local copies, waits for them, and re-layouts: 25 us -> 2.58 us
  other arithmetic: 14.1 us -> 1.19 us
  matrix products: 9.06 us -> 0 us
  blocking collectives: 5.16 us -> 0 us
    pallas_call x0 -> x1, Pallas kernels: none -> 61.9 us  [shards(): pl.pallas_call(functools.partial(kernel, sizes), out_shape=(shape((owned,...]
    all_to_all x5 -> x0, waiting for transfers between devices: 42.3 us -> none  [the longest x1 13.8 us: shards(): lax.all_to_all(middle_rows, EP, split_axis=1, concat_axis=0, tiled=True)]
    all_to_all x5 -> x0, starting transfers between devices: 37.7 us -> none  [the longest x1 19 us: shards(): lax.all_to_all(middle_rows, EP, split_axis=1, concat_axis=0, tiled=True)]
    reduce_sum x10 -> x0, other arithmetic: 9.65 us -> none  [the longest x1 5.62 us: shards(): jnp.sum(picked * weights[:, :, None], axis=1)]
    dot_general x10 -> x0, matrix products: 9.06 us -> none  [the longest x1 1.45 us: shards(): jnp.einsum('ecf,efd->ecd', activation, w_down, preferred_element_type=jnp...]
    gather x1 -> x0, local copies, waits for them, and re-layouts: 6.18 us -> none  [shards(): returned.reshape(expert_count * EXPERT_CAPACITY, col_count)[targets]]
    scatter x1 -> x0, local copies, waits for them, and re-layouts: 6.07 us -> none  [shards(): buffer = jnp.zeros((expert_count * EXPERT_CAPACITY, col_count), jnp.bfloa...]
    all_to_all x1 -> x0, blocking collectives: 5.16 us -> none  [exchange_in_order(): lax.all_to_all(pieces, axes[k], split_axis=k, concat_axis=k, tiled=True)]
  transfers between devices with their start and end apart: 5 -> 0, of which waited for: 5 -> 0; matrix products, arithmetic and copies ran while one was open for 3% -> 0% of each run, Pallas kernels for 0% -> 0%
where the time goes in v1:
time: 66.5 us; the launch traced here: 66.3 us
  Pallas kernels  61.9 us (93%)
  local copies, waits for them, and re-layouts  2.58 us (4%)
  other arithmetic  1.19 us (2%)
  between operations  0.71 us (1%)
    pallas_call x1, Pallas kernels, shards(): pl.pallas_call(functools.partial(kernel, sizes), out_shape=(shape((owned,...  61.9 us
    unnamed x17, local copies, waits for them, and re-layouts  2.46 us

profile of v1, /device:TPU:1, one launch (start us, length us, event | category | flops | bytes accessed | tf_op | source)
XLA Modules:
  0.0 66.3 jit_solution(9121227728187415736)
XLA Ops:
  0.6 0.0 copy-start
  0.6 61.9 %shard_map.219 = (bf16[8,1024]{1,0:T(8,128)(2,1)}, f32[8,128]{1,0:T(8,128)}, f32[8,128]{1,0:T(8,128)}, f32[8,256]{1,0:T(8,128)}, f32[8,128]{1,0:T(8,128)}, /*index=5*/f32[1,8]{1,0:T(1,128)}) custom-call(bf16[8,1024]{1,0:T(8,128)(2,1)} %tok_h.1, f32[1,1024]{1,0:T(1,128)} %bitcast.29, bf16[1024,128]{1,0:T(8,128)(2,1)} %wq_h.1, bf16[1024,128]{1,0:T(8,128)(2,1)} %wk_h.1, ...), custom_call_target="tpu_custom_call" | custom-call | tf_op jit(solution)/shard_map/pallas_call | solution.py:505
  62.5 0.0 copy-start.4
  62.5 0.0 copy-start.2
  62.5 0.0 copy-start.3
  62.6 0.6 copy-done.4
  63.2 0.1 slice_reduce_fusion
  63.3 0.0 copy-done
  63.3 0.0 copy-done.2
  63.3 0.0 copy-done.3
  63.3 0.0 copy-start.1
  63.3 1.2 %multiply_add_fusion = f32[8,1,128,256]{3,2,1,0:T(8,128)} fusion(f32[8,1,128,256]{3,2,1,0:T(8,128)S(1)} %copy-done, f32[8,256]{1,0:T(8,128)S(1)} %copy-done.2, f32[8,128]{1,0:T(8,128)S(1)} %copy-done.3, f32[8]{0:T(128)S(1)} %slice_reduce_fusion), kind=kLoop, calls=%fused_computation | loop fusion | flops 786432 | bytes 2109472 | tf_op jit(solution)/shard_map/add | solution.py:541
  64.5 0.0 copy-done.1
  64.5 0.0 copy-start.5
  64.5 0.6 copy.29
  65.1 0.1 copy-done.5
  65.2 0.0 copy-start.6
  65.2 0.6 copy.30
  65.8 0.0 copy-done.6
  65.8 0.5 copy.31
Async XLA Ops:
  0.6 62.7 %copy-start = (f32[8,1,128,256]{3,2,1,0:T(8,128)S(1)}, f32[8,1,128,256]{3,2,1,0:T(8,128)}, u32[]{:S(2)}) copy-start(f32[8,1,128,256]{3,2,1,0:T(8,128)} %param.31) | copy-start | bytes 3145732
  62.5 0.7 %copy-start.4 = (f32[8,128]{1,0:T(8,128)S(1)}, f32[8,128]{1,0:T(8,128)}, u32[]{:S(2)}) copy-start(f32[8,128]{1,0:T(8,128)} %get-tuple-element.11) | copy-start | bytes 12292
  62.5 0.8 %copy-start.2 = (f32[8,256]{1,0:T(8,128)S(1)}, f32[8,256]{1,0:T(8,128)}, u32[]{:S(2)}) copy-start(f32[8,256]{1,0:T(8,128)} %get-tuple-element.13) | copy-start | bytes 24580
  62.5 0.8 %copy-start.3 = (f32[8,128]{1,0:T(8,128)S(1)}, f32[8,128]{1,0:T(8,128)}, u32[]{:S(2)}) copy-start(f32[8,128]{1,0:T(8,128)} %get-tuple-element.12) | copy-start | bytes 12292
  63.3 1.2 %copy-start.1 = (bf16[8,1024]{1,0:T(8,128)(2,1)S(1)}, bf16[8,1024]{1,0:T(8,128)(2,1)}, u32[]{:S(2)}) copy-start(bf16[8,1024]{1,0:T(8,128)(2,1)} %get-tuple-element.10) | copy-start | bytes 49156
  64.5 0.7 %copy-start.5 = (f32[8,128]{1,0:T(8,128)S(1)}, f32[8,128]{1,0:T(8,128)}, u32[]{:S(2)}) copy-start(f32[8,128]{1,0:T(8,128)} %get-tuple-element.14) | copy-start | bytes 12292
  65.2 0.6 copy-start.6

commit v2 on v1

--- a/solution.py
+++ b/solution.py
@@ -38,16 +38,13 @@
     rmax_h,
     fg_h,
     route_h,
-    rw_h,
     wgate_h,
     wup_h,
     wdown_h,
-    mixed_ref,
-    keep_ref,
-    akey_ref,
-    value_ref,
-    newnorm_ref,
-    newmax_ref,
+    frecv,
+    mrecv,
+    tgt_ref,
+    pack_ref,
     tok,
     mix,
     wq,
@@ -64,12 +61,12 @@
     rmax,
     fg,
     route,
-    rw,
     wgate,
     wup,
     wdown,
     load_sem,
     tgt,
+    pack,
     place,
     psend,
     precv,
@@ -79,14 +76,15 @@
     erecv,
     rsend,
     rrecv,
-    stage,
+    msend,
     dsend,
-    frecv,
     psem,
     csem,
     esem,
     rsem,
+    msem,
     dsem,
+    out_sem,
 ):
     nz, ny, nc, nx = sizes
     z, y, c, x = (lax.axis_index(a) for a in ("z", "y", "c", "x"))
@@ -102,31 +100,33 @@
     expert_count = chips * nc
     token_count = route.shape[1]
 
-    hbm = (tok_h, mix_h, wq_h, wk_h, wv_h, wo_h, wi_h, wf_h, fb_h, hg_h, wout_h, mem_h, nrm_h, rmax_h)
-    hbm += (fg_h, route_h, rw_h, wgate_h, wup_h, wdown_h)
-    vmem = (tok, mix, wq, wk, wv, wo, wi, wf, fb, hg, wout, mem, nrm, rmax)
-    vmem += (fg, route, rw, wgate, wup, wdown)
-    loads = [pltpu.make_async_copy(h, v, load_sem.at[i]) for i, (h, v) in enumerate(zip(hbm, vmem))]
-    for load in loads:
-        load.start()
-
     barrier = pltpu.get_barrier_semaphore()
 
     def greet(target):
         pl.semaphore_signal(barrier, inc=1, device_id=target, device_id_type=MESH)
 
+    y_order = sorted(range(ny), key=lambda d: -min(d, ny - d))
+
+    def ring_z(i):
+        shift = nz // 2 + jnp.where(i % 2 == 0, i // 2, -((i + 1) // 2))
+        return lax.rem(z + shift, nz)
+
     def greet_plane(i, carry):
-        tz, ty = lax.rem(z + i // ny, nz), lax.rem(y + i % ny, ny)
-
-        @pl.when(i > 0)
-        def _():
-            greet((tz, ty, c, x))
-
-        for dc in range(1, nc):
-            greet((tz, ty, lax.rem(c + dc, nc), x))
+        tz = ring_z(i)
+        for dy in y_order:
+            ty = lax.rem(y + dy, ny)
+            for dc in reversed(range(nc)):
+                tc = lax.rem(c + dc, nc)
+                if dy == 0 and dc == 0:
+
+                    @pl.when(i < nz - 1)
+                    def _():
+                        greet((tz, ty, tc, x))
+                else:
+                    greet((tz, ty, tc, x))
         return carry
 
-    lax.fori_loop(0, chips, greet_plane, 0)
+    lax.fori_loop(0, nz, greet_plane, 0)
     for dx in range(1, nx):
         for dc in range(nc):
             greet((z, y, lax.rem(c + dc, nc), lax.rem(x + dx, nx)))
@@ -134,16 +134,13 @@
     source_x, source_c = source_group // nc, source_group % nc
     from_self = source_group == group
 
-    def greet_sources(i, carry):
-        tz, ty = lax.rem(z + i // ny, nz), lax.rem(y + i % ny, ny)
-
-        @pl.when(jnp.logical_or(i > 0, jnp.logical_not(from_self)))
-        def _():
-            greet((tz, ty, source_c, source_x))
-
-        return carry
-
-    lax.fori_loop(0, chips, greet_sources, 0)
+    hbm = (tok_h, mix_h, wq_h, wk_h, wv_h, wo_h, wi_h, wf_h, fb_h, hg_h, wout_h, mem_h, nrm_h, rmax_h)
+    hbm += (fg_h, route_h, wgate_h, wup_h, wdown_h)
+    vmem = (tok, mix, wq, wk, wv, wo, wi, wf, fb, hg, wout, mem, nrm, rmax)
+    vmem += (fg, route, wgate, wup, wdown)
+    loads = [pltpu.make_async_copy(h, v, load_sem.at[i]) for i, (h, v) in enumerate(zip(hbm, vmem))]
+    for load in loads:
+        load.start()
 
     for i in range(14):
         loads[i].wait()
@@ -152,8 +149,7 @@
     normed = (tokens * lax.rsqrt(mean + EPS) * mix[...]).astype(BF16)
     query16 = dot(normed, wq[...]).astype(BF16)
     query = query16.astype(F32)
-    qk = wq.shape[1]
-    scaled_key = dot(normed, wk[...]).astype(BF16).astype(F32) * qk ** (-0.5)
+    scaled_key = dot(normed, wk[...]).astype(BF16).astype(F32) * wq.shape[1] ** (-0.5)
     value = dot(normed, wv[...]).astype(BF16).astype(F32)
     ogate = dot(normed, wo[...]).astype(BF16).astype(F32)
     floats = normed.astype(F32)
@@ -177,13 +173,13 @@
     admit = jnp.exp(log_in - new_max)
     akey = admit * scaled_key
     norm_state = keep * nrm[...] + akey
-    keep_ref[...] = jnp.broadcast_to(keep, keep_ref.shape)
-    akey_ref[...] = akey
-    value_ref[...] = value
-    newnorm_ref[...] = norm_state
-    newmax_ref[...] = jnp.sum(
-        jnp.where(diagonal, jnp.broadcast_to(new_max, (rows, rows)), 0.0), axis=0, keepdims=True
-    )
+    qk = wq.shape[1]
+    dv = wv.shape[1]
+    pack[:, 0:LANES] = jnp.broadcast_to(keep, (rows, LANES))
+    pack[:, LANES : LANES + qk] = akey
+    pack[:, LANES + qk : LANES + qk + dv] = value
+    pack[:, LANES + qk + dv : LANES + 2 * qk + dv] = norm_state
+    pack[:, LANES + 2 * qk + dv :] = jnp.broadcast_to(new_max, (rows, LANES))
     row_of = lax.broadcasted_iota(jnp.int32, value.shape, 0)
     kept = jnp.zeros_like(value)
     for t in range(rows):
@@ -220,9 +216,14 @@
     slot_id = lax.broadcasted_iota(jnp.int32, (slots_here, token_count), 0) + zy * slots_here
     hit = jnp.logical_or(slot_id == tgt[0:1, :], slot_id == tgt[1:2, :])
     place[...] = jnp.where(hit, 1.0, 0.0).astype(BF16)
-
-    own_target = jnp.where(from_self, 1, 0)
-    pl.semaphore_wait(barrier, chips * nc - 1 + (nx - 1) * nc + owners * nx - own_target)
+    keeps = [
+        pltpu.make_async_copy(tgt, tgt_ref, out_sem.at[0]),
+        pltpu.make_async_copy(pack, pack_ref, out_sem.at[1]),
+    ]
+    for copy in keeps:
+        copy.start()
+
+    pl.semaphore_wait(barrier, chips * nc - 1 + (nx - 1) * nc)
 
     for dx in range(1, nx):
         tx = lax.rem(x + dx, nx)
@@ -252,9 +253,9 @@
         csend[i] = middle[:, i * LANES : (i + 1) * LANES]
 
     def send_plane(i, carry):
-        tz, ty = lax.rem(z + i // ny, nz), lax.rem(y + i % ny, ny)
-
-        def send(tc):
+        tz = ring_z(i)
+
+        def send(ty, tc):
             pltpu.make_async_remote_copy(
                 src_ref=csend.at[tc],
                 dst_ref=crecv.at[ep],
@@ -264,16 +265,20 @@
                 device_id_type=MESH,
             ).start()
 
-        for dc in range(1, nc):
-            send(lax.rem(c + dc, nc))
-
-        @pl.when(i > 0)
-        def _():
-            send(c)
-
+        for dy in y_order:
+            ty = lax.rem(y + dy, ny)
+            for dc in reversed(range(nc)):
+                tc = lax.rem(c + dc, nc)
+                if dy == 0 and dc == 0:
+
+                    @pl.when(i < nz - 1)
+                    def _():
+                        send(ty, tc)
+                else:
+                    send(ty, tc)
         return carry
 
-    lax.fori_loop(0, chips, send_plane, 0)
+    lax.fori_loop(0, nz, send_plane, 0)
     crecv[ep] = csend[c]
     others = crecv.at[pl.ds(0, chips * nc - 1)]
     plane = pltpu.make_async_remote_copy(
@@ -285,8 +290,8 @@
         device_id_type=MESH,
     )
     plane.wait_recv()
-    everyone = crecv[...].astype(F32).reshape(token_count, LANES).astype(BF16)
-    slots = dot(place[...], everyone).astype(BF16)
+    everyone32 = crecv[...].astype(F32).reshape(token_count, LANES)
+    slots = dot(place[...], everyone32.astype(BF16)).astype(BF16)
     for i in range(nc):
         esend[i] = slots[i * CAP : (i + 1) * CAP]
 
@@ -312,7 +317,15 @@
 
     to_experts = chip_row(esend, erecv, esem, lambda tx, tc: tc, group)
     erecv[group] = esend[c]
-    for i in (14, 17, 18, 19):
+
+    @pl.when(from_self)
+    def _():
+        turned = everyone32.T
+        for k in range(owners):
+            msend[k] = turned[k * owned : (k + 1) * owned, :].astype(BF16)
+        pltpu.make_async_copy(msend.at[lax.rem(ep, owners)], mrecv, out_sem.at[2]).start()
+
+    for i in (14, 16, 17, 18):
         loads[i].wait()
     for copy in to_experts:
         copy.wait_recv()
@@ -328,42 +341,68 @@
 
     to_groups = chip_row(rsend, rrecv, rsem, lambda tx, tc: tx * nc + tc, group)
     rrecv[group] = rsend[group]
-    stage[slots_here:, :] = jnp.zeros((LANES - slots_here, LANES), F32)
-    here = nc * rows
-    spot = pl.multiple_of(slots_here + lax.rem(zy, 4) * here, here)
-    stage[pl.ds(spot, here), :] = crecv[pl.ds(zy * nc, nc)].astype(F32).reshape(here, LANES)
+
+    middle_copies = []
+    for dx in range(nx):
+        for dc in range(nc):
+            if dx + dc > 0:
+                tx, tc = lax.rem(x + dx, nx), lax.rem(c + dc, nc)
+                copy = pltpu.make_async_remote_copy(
+                    src_ref=msend.at[lax.rem(y * nc + tc, owners)],
+                    dst_ref=mrecv,
+                    send_sem=msem.at[0],
+                    recv_sem=msem.at[1],
+                    device_id=(z, y, tc, tx),
+                    device_id_type=MESH,
+                )
+                middle_copies.append(copy)
+
+    @pl.when(from_self)
+    def _():
+        for copy in middle_copies:
+            copy.start()
+
     for copy in to_groups:
         copy.wait_recv()
+    results = []
     for i in range(nc):
         result = rrecv[i].astype(F32)
         for j in range(1, nx):
             result = result + rrecv[j * nc + i].astype(F32)
-        stage[i * CAP : (i + 1) * CAP, :] = result
-    dsend[...] = stage[...].T.reshape(owners, owned, LANES).astype(BF16)
-
-    count = owners * nx
-
-    def send_owner(i, carry):
-        n = lax.rem(i + zy, count)
-        k, tx = n // nx, n % nx
-        target = group * owners + k
-        tc = target % nc
-        tzy = target // nc
-
-        @pl.when(jnp.logical_not(jnp.logical_and(target == ep, tx == x)))
-        def _():
+        results.append(result)
+    low = lax.broadcasted_iota(jnp.int32, (owners, owned // 2, LANES), 2) < slots_here
+    turned = jnp.concatenate(results + results, axis=0).T.reshape(owners, owned, LANES)
+    half = owned // 2
+    dsend[...] = jnp.where(low, turned[:, :half], turned[:, half:]).astype(BF16)
+
+    def send_owners(i, carry):
+        shift = ny // 2 + jnp.where(i % 2 == 0, i // 2, -((i + 1) // 2))
+        ty = lax.rem(y + shift, ny)
+
+        def send(tc, tx):
             pltpu.make_async_remote_copy(
-                src_ref=dsend.at[k],
+                src_ref=dsend.at[ty * nc + tc],
                 dst_ref=frecv.at[zy],
                 send_sem=dsem.at[0],
                 recv_sem=dsem.at[1],
-                device_id=(tzy // ny, tzy % ny, tc, tx),
+                device_id=(group, ty, tc, tx),
                 device_id_type=MESH,
             ).start()
 
+        for dx in sorted(range(nx), key=lambda d: -min(d, nx - d)):
+            tx = lax.rem(x + dx, nx)
+            for dc in reversed(range(nc)):
+                tc = lax.rem(c + dc, nc)
+                if dx == 0 and dc == 0:
+
+                    @pl.when(jnp.logical_not(jnp.logical_and(from_self, i == ny - 1)))
+                    def _():
+                        send(tc, tx)
+                else:
+                    send(tc, tx)
         return carry
 
-    lax.fori_loop(0, count, send_owner, 0)
+    lax.fori_loop(0, ny, send_owners, 0)
 
     def arrivals(n):
         part = frecv.at[pl.ds(0, n)]
@@ -376,53 +415,21 @@
             device_id_type=MESH,
         )
 
-    loads[16].wait()
-
     @pl.when(from_self)
     def _():
-        frecv[zy] = dsend[lax.rem(ep, owners)]
+        own = pltpu.make_async_copy(dsend.at[lax.rem(ep, owners)], frecv.at[zy], out_sem.at[3])
+        own.start()
         arrivals(chips - 1).wait_recv()
+        own.wait()
+        pltpu.make_async_copy(msend.at[lax.rem(ep, owners)], mrecv, out_sem.at[2]).wait()
 
     @pl.when(jnp.logical_not(from_self))
     def _():
+        middle_copies[0].wait_recv()
         arrivals(chips).wait_recv()
 
-    vregs = token_count // LANES
-    lane = lax.broadcasted_iota(jnp.int32, (owned, LANES), 1)
-    low = lane < slots_here
-    names = []
-    for j in range(2):
-        for k in range(vregs):
-            t = jnp.broadcast_to(tgt[j : j + 1, k * LANES : (k + 1) * LANES], (owned, LANES))
-            names.append((jnp.bitwise_and(t, LANES - 1), lax.shift_right_logical(t, 7)))
-
-    def pick(p, found):
-        second = pltpu.roll(frecv[2 * p + 1].astype(F32), slots_here, 1)
-        held = jnp.where(low, frecv[2 * p].astype(F32), second)
-        return tuple(
-            jnp.where(
-                part == p,
-                jnp.take_along_axis(held, index, axis=1, mode="promise_in_bounds"),
-                f,
-            )
-            for f, (index, part) in zip(found, names)
-        )
-
-    nothing = jnp.zeros((owned, LANES), F32)
-    found = lax.fori_loop(0, chips // 2, pick, (nothing,) * (2 * vregs))
-    for k in range(vregs):
-        halves = []
-        for h in range(2):
-            half = frecv[8 * k + 4 * h].astype(F32)
-            for m in range(1, 4):
-                half = half + frecv[8 * k + 4 * h + m].astype(F32)
-            halves.append(half)
-        mid = jnp.where(low, pltpu.roll(halves[0], slots_here, 1), halves[1])
-        w0 = rw[0:1, k * LANES : (k + 1) * LANES]
-        w1 = rw[1:2, k * LANES : (k + 1) * LANES]
-        both = w0 + w1
-        mixed = mid + (found[k] * (w0 / both) + found[vregs + k] * (w1 / both))
-        mixed_ref[:, k * LANES : (k + 1) * LANES] = mixed.astype(BF16)
+    for copy in keeps:
+        copy.wait()
 
     for dx in range(1, nx):
         pltpu.make_async_remote_copy(
@@ -439,11 +446,103 @@
 
     @pl.when(from_self)
     def _():
-        arrivals(count - 1).wait_send()
+        for copy in middle_copies:
+            copy.wait_send()
+        arrivals(chips - 1).wait_send()
 
     @pl.when(jnp.logical_not(from_self))
     def _():
-        arrivals(count).wait_send()
+        arrivals(chips).wait_send()
+
+
+def combine(
+    parts_h,
+    mid_h,
+    tgt_h,
+    rw_h,
+    pack_h,
+    mem_h,
+    mixed_ref,
+    newmem_ref,
+    newnorm_ref,
+    newmax_ref,
+    parts,
+    mid,
+    tgt,
+    rw,
+    pack,
+    mem,
+    state,
+    load_sem,
+    mem_sem,
+    sem,
+):
+    rows, qk, dv = mem.shape
+    chips, half, _ = parts.shape
+    owned = 2 * half
+    token_count = tgt.shape[1]
+    loads = []
+    for i, (h, v) in enumerate(
+        ((pack_h, pack), (tgt_h, tgt), (parts_h, parts), (mid_h, mid), (rw_h, rw))
+    ):
+        loads.append(pltpu.make_async_copy(h, v, load_sem.at[i]))
+    mem_loads = [pltpu.make_async_copy(mem_h.at[t], mem.at[t], mem_sem.at[t]) for t in range(rows)]
+    for copy in loads + mem_loads:
+        copy.start()
+    loads[0].wait()
+    copies = []
+    value = pack[:, LANES + qk : LANES + qk + dv]
+    for t in range(rows):
+        key_columns = jnp.broadcast_to(pack[t : t + 1, LANES : LANES + qk], (LANES, LANES)).T
+        key_columns = jnp.concatenate([key_columns] * (dv // LANES), axis=1)
+        mem_loads[t].wait()
+        state[t] = pack[t : t + 1, 0:1] * mem[t] + key_columns * value[t : t + 1, :]
+        copy = pltpu.make_async_copy(state.at[t], newmem_ref.at[t], sem.at[t])
+        copy.start()
+        copies.append(copy)
+    newnorm_ref[...] = pack[:, LANES + qk + dv : LANES + 2 * qk + dv]
+    diagonal = lax.broadcasted_iota(jnp.int32, (rows, LANES), 0) == lax.broadcasted_iota(
+        jnp.int32, (rows, LANES), 1
+    )
+    row = jnp.where(diagonal, pack[:, LANES + 2 * qk + dv :], 0.0)
+    newmax_ref[...] = jnp.sum(row, axis=0, keepdims=True)[:, :rows]
+    for copy in loads[1:]:
+        copy.wait()
+
+    low = lax.broadcasted_iota(jnp.int32, (chips // 2, half, LANES), 2) < LANES // 2
+    both = parts[...].astype(F32).reshape(chips // 2, 2, half, LANES)
+    even, odd = both[:, 0], both[:, 1]
+    even_turned = pltpu.roll(even, LANES // 2, 2)
+    odd_turned = pltpu.roll(odd, LANES // 2, 2)
+    held = jnp.concatenate(
+        [jnp.where(low, even, odd_turned), jnp.where(low, even_turned, odd)], axis=1
+    )
+    held = held.reshape(chips // 2 * owned, LANES).astype(BF16)
+    lane_id = lax.broadcasted_iota(jnp.int32, (LANES, LANES), 0)
+    for k in range(token_count // LANES):
+        span = slice(k * LANES, (k + 1) * LANES)
+        names = [tgt[j : j + 1, span] for j in range(2)]
+        picks = jnp.concatenate(
+            [
+                jnp.where(lane_id == jnp.bitwise_and(n, LANES - 1), 1.0, 0.0).astype(BF16)
+                for n in names
+            ],
+            axis=1,
+        )
+        found = dot(held, picks)
+        total = []
+        for j in range(2):
+            place = jnp.broadcast_to(lax.shift_right_logical(names[j], 7), (owned, LANES))
+            got = jnp.zeros((owned, LANES), F32)
+            for p in range(chips // 2):
+                part = found[p * owned : (p + 1) * owned, j * LANES : (j + 1) * LANES]
+                got = jnp.where(place == p, part, got)
+            total.append(got)
+        w0, w1 = rw[0:1, span], rw[1:2, span]
+        weighed = total[0] * (w0 / (w0 + w1)) + total[1] * (w1 / (w0 + w1))
+        mixed_ref[:, span] = (mid[:, span].astype(F32) + weighed).astype(BF16)
+    for copy in copies:
+        copy.wait()
 
 
 def shards(
@@ -495,29 +594,29 @@
         running_max.T,
         ffn_gain.reshape(1, -1),
         route.T,
-        route_weight.T,
         w_gate[0],
         w_up[0],
         w_down[0],
     )
     shape = jax.ShapeDtypeStruct
     vmem = pl.BlockSpec(memory_space=pltpu.VMEM)
-    mixed, keep, akey, value, new_norm, new_max = pl.pallas_call(
+    hbm = pl.BlockSpec(memory_space=pl.ANY)
+    pack_width = LANES * 2 + 2 * qk + dv
+    parts, mid, tgt, pack = pl.pallas_call(
         functools.partial(kernel, sizes),
         out_shape=(
+            shape((chips, owned // 2, LANES), BF16),
             shape((owned, token_count), BF16),
-            shape((rows, LANES), F32),
-            shape((rows, qk), F32),
-            shape((rows, dv), F32),
-            shape((rows, qk), F32),
-            shape((1, rows), F32),
+            shape((2, token_count), jnp.int32),
+            shape((rows, pack_width), F32),
         ),
-        in_specs=[pl.BlockSpec(memory_space=pl.ANY)] * len(operands),
-        out_specs=(vmem,) * 6,
+        in_specs=[hbm] * len(operands),
+        out_specs=(hbm,) * 4,
         scratch_shapes=[pltpu.VMEM(a.shape, a.dtype) for a in operands]
         + [
             pltpu.SemaphoreType.DMA((len(operands),)),
             pltpu.VMEM((2, token_count), jnp.int32),
+            pltpu.VMEM((rows, pack_width), F32),
             pltpu.VMEM((nc * CAP, token_count), BF16),
             pltpu.VMEM((nx, rows, quarter), BF16),
             pltpu.VMEM((nx - 1, rows, quarter), BF16),
@@ -527,29 +626,49 @@
             pltpu.VMEM((groups, CAP, LANES), BF16),
             pltpu.VMEM((groups, CAP, LANES), BF16),
             pltpu.VMEM((groups, CAP, LANES), BF16),
-            pltpu.VMEM((LANES, LANES), F32),
-            pltpu.VMEM((owners, owned, LANES), BF16),
-            pltpu.VMEM((max(chips, owners * nx), owned, LANES), BF16),
+            pltpu.VMEM((owners, owned, token_count), BF16),
+            pltpu.VMEM((owners, owned // 2, LANES), BF16),
             pltpu.SemaphoreType.DMA((2, nx - 1)),
             pltpu.SemaphoreType.DMA((2,)),
             pltpu.SemaphoreType.DMA((2, groups - 1)),
             pltpu.SemaphoreType.DMA((2, groups - 1)),
             pltpu.SemaphoreType.DMA((2,)),
+            pltpu.SemaphoreType.DMA((2,)),
+            pltpu.SemaphoreType.DMA((4,)),
         ],
         compiler_params=pltpu.CompilerParams(collective_id=0, has_side_effects=True),
     )(*operands)
-    state = keep[:, :1, None] * memory[:, 0] + akey[:, :, None] * value[:, None, :]
+    mixed, state, new_norm, new_max = pl.pallas_call(
+        combine,
+        out_shape=(
+            shape((owned, token_count), BF16),
+            shape((rows, qk, dv), F32),
+            shape((rows, qk), F32),
+            shape((1, rows), F32),
+        ),
+        in_specs=[hbm] * 6,
+        out_specs=(vmem, hbm, vmem, vmem),
+        scratch_shapes=[
+            pltpu.VMEM((chips, owned // 2, LANES), BF16),
+            pltpu.VMEM((owned, token_count), BF16),
+            pltpu.VMEM((2, token_count), jnp.int32),
+            pltpu.VMEM((2, token_count), F32),
+            pltpu.VMEM((rows, pack_width), F32),
+            pltpu.VMEM((rows, qk, dv), F32),
+            pltpu.VMEM((rows, qk, dv), F32),
+            pltpu.SemaphoreType.DMA((5,)),
+            pltpu.SemaphoreType.DMA((rows,)),
+            pltpu.SemaphoreType.DMA((rows,)),
+        ],
+    )(parts, mid, tgt, route_weight.T, pack, memory.reshape(rows, qk, dv))
     return (mixed.T, state[:, None], new_norm[:, None], new_max.T)
 
 
 def solution(mesh):
     nx = mesh.shape["tp"]
     nc = 2
-    nz = mesh.shape["ep"] // nc
-    ny = 1
-    while ny * ny < nz:
-        ny *= 2
-    nz //= ny
+    nz = nx * nc
+    ny = mesh.shape["ep"] // (nc * nz)
     finer = Mesh(mesh.devices.reshape(nz, ny, nc, nx), ("z", "y", "c", "x"))
     ep = ("z", "y", "c")
     in_specs = (

time: 66.5 us -> 50.4 us (0.76)
  Pallas kernels: 61.9 us -> 49.6 us
  local copies, waits for them, and re-layouts: 2.58 us -> 0 us
  other arithmetic: 1.19 us -> 0 us
    pallas_call x1 -> x2, Pallas kernels: 61.9 us -> 49.6 us  [the longest x1 46.2 us: shards(): pl.pallas_call(functools.partial(kernel, sizes), out_shape=(shape((chips,...]
    unnamed x17 -> x0, local copies, waits for them, and re-layouts: 2.46 us -> none
    add x1 -> x0, other arithmetic: 1.19 us -> none  [shards(): keep[:, :1, None] * memory[:, 0] + akey[:, :, None] * value[:, None, :]]
where the time goes in v2:
time: 50.4 us; the launch traced here: 50.2 us
  Pallas kernels  49.6 us (98%)
  between operations  0.65 us (1%)
    pallas_call x1, Pallas kernels, shards(): pl.pallas_call(functools.partial(kernel, sizes), out_shape=(shape((chips,...  46.2 us
    pallas_call x1, Pallas kernels, shards(): pl.pallas_call(combine, out_shape=(shape((owned, token_count), BF16), sha...  3.38 us

profile of v2, /device:TPU:1, one launch (start us, length us, event | category | flops | bytes accessed | tf_op | source)
XLA Modules:
  0.0 50.2 jit_solution(4407387431424015665)
XLA Ops:
  0.6 46.2 %shard_map.219 = (bf16[64,4,128]{2,1,0:T(4,128)(2,1)}, bf16[8,1024]{1,0:T(8,128)(2,1)}, s32[2,1024]{1,0:T(2,128)}, f32[8,768]{1,0:T(8,128)}) custom-call(bf16[8,1024]{1,0:T(8,128)(2,1)} %tok_h.1, f32[1,1024]{1,0:T(1,128)} %bitcast.31, bf16[1024,128]{1,0:T(8,128)(2,1)} %wq_h.1, bf16[1024,128]{1,0:T(8,128)(2,1)} %wk_h.1, bf16[1024,256]{1,0:T(8,128)(2,1)} %wv_h.1, ...), custom_call_target="tpu_custom_call" | custom-call | tf_op jit(solution)/shard_map/pallas_call | solution.py:605
  46.9 3.4 %shard_map.220 = (bf16[8,1024]{1,0:T(8,128)(2,1)}, f32[8,128,256]{2,1,0:T(8,128)}, f32[8,128]{1,0:T(8,128)}, f32[1,8]{1,0:T(1,128)}) custom-call(bf16[64,4,128]{2,1,0:T(4,128)(2,1)} %get-tuple-element.12.parts_h, bf16[8,1024]{1,0:T(8,128)(2,1)} %get-tuple-element.13.mid_h, s32[2,1024]{1,0:T(2,128)} %get-tuple-element.14.tgt_h, f32[2,1024]{1,0:T(2,128)} %bitcast.30, ...), custom_call_target="tpu_custom_call" | custom-call | tf_op jit(solution)/shard_map/pallas_call | solution.py:641

commit v3 on v2

--- a/solution.py
+++ b/solution.py
@@ -45,6 +45,7 @@
     mrecv,
     tgt_ref,
     pack_ref,
+    state_ref,
     tok,
     mix,
     wq,
@@ -85,6 +86,8 @@
     msem,
     dsem,
     out_sem,
+    plane_sem,
+    state,
 ):
     nz, ny, nc, nx = sizes
     z, y, c, x = (lax.axis_index(a) for a in ("z", "y", "c", "x"))
@@ -111,25 +114,17 @@
         shift = nz // 2 + jnp.where(i % 2 == 0, i // 2, -((i + 1) // 2))
         return lax.rem(z + shift, nz)
 
-    def greet_plane(i, carry):
-        tz = ring_z(i)
-        for dy in y_order:
-            ty = lax.rem(y + dy, ny)
-            for dc in reversed(range(nc)):
-                tc = lax.rem(c + dc, nc)
-                if dy == 0 and dc == 0:
-
-                    @pl.when(i < nz - 1)
-                    def _():
-                        greet((tz, ty, tc, x))
-                else:
-                    greet((tz, ty, tc, x))
-        return carry
-
-    lax.fori_loop(0, nz, greet_plane, 0)
-    for dx in range(1, nx):
+    z_order = sorted(range(1, nz), key=lambda d: -min(d, nz - d))
+    for dz in z_order:
+        tz = lax.rem(z + dz, nz)
         for dc in range(nc):
-            greet((z, y, lax.rem(c + dc, nc), lax.rem(x + dx, nx)))
+            greet((tz, y, lax.rem(c + dc, nc), x))
+    for dy in y_order[:-1]:
+        greet((z, lax.rem(y + dy, ny), c, x))
+    for dx in range(nx):
+        for dc in range(nc):
+            if dx + dc > 0:
+                greet((z, y, lax.rem(c + dc, nc), lax.rem(x + dx, nx)))
     source_group = ep // owners
     source_x, source_c = source_group // nc, source_group % nc
     from_self = source_group == group
@@ -174,12 +169,8 @@
     akey = admit * scaled_key
     norm_state = keep * nrm[...] + akey
     qk = wq.shape[1]
-    dv = wv.shape[1]
-    pack[:, 0:LANES] = jnp.broadcast_to(keep, (rows, LANES))
-    pack[:, LANES : LANES + qk] = akey
-    pack[:, LANES + qk : LANES + qk + dv] = value
-    pack[:, LANES + qk + dv : LANES + 2 * qk + dv] = norm_state
-    pack[:, LANES + 2 * qk + dv :] = jnp.broadcast_to(new_max, (rows, LANES))
+    pack[:, 0:qk] = norm_state
+    pack[:, qk:] = jnp.broadcast_to(new_max, (rows, LANES))
     row_of = lax.broadcasted_iota(jnp.int32, value.shape, 0)
     kept = jnp.zeros_like(value)
     for t in range(rows):
@@ -192,6 +183,23 @@
     partial = dot(gated, wout[...]).astype(BF16)
     for i in range(nx):
         psend[i] = partial[:, i * quarter : (i + 1) * quarter]
+    pl.semaphore_wait(barrier, (nz - 1) * nc + ny - 1 + nx * nc - 1)
+
+    for dy in y_order[:-1]:
+        pl.semaphore_signal(
+            plane_sem, inc=1, device_id=(z, lax.rem(y + dy, ny), c, x), device_id_type=MESH
+        )
+
+    for dx in range(1, nx):
+        tx = lax.rem(x + dx, nx)
+        pltpu.make_async_remote_copy(
+            src_ref=psend.at[tx],
+            dst_ref=precv.at[dx - 1],
+            send_sem=psem.at[0, dx - 1],
+            recv_sem=psem.at[1, dx - 1],
+            device_id=(z, y, c, tx),
+            device_id_type=MESH,
+        ).start()
 
     loads[15].wait()
     expert_of = lax.broadcasted_iota(jnp.int32, (expert_count, token_count), 0)
@@ -223,18 +231,6 @@
     for copy in keeps:
         copy.start()
 
-    pl.semaphore_wait(barrier, chips * nc - 1 + (nx - 1) * nc)
-
-    for dx in range(1, nx):
-        tx = lax.rem(x + dx, nx)
-        pltpu.make_async_remote_copy(
-            src_ref=psend.at[tx],
-            dst_ref=precv.at[dx - 1],
-            send_sem=psem.at[0, dx - 1],
-            recv_sem=psem.at[1, dx - 1],
-            device_id=(z, y, c, tx),
-            device_id_type=MESH,
-        ).start()
     total = psend[x].astype(F32)
     for dx in range(1, nx):
         copy = pltpu.make_async_remote_copy(
@@ -278,8 +274,16 @@
                     send(ty, tc)
         return carry
 
+    pl.semaphore_wait(plane_sem, ny - 1)
     lax.fori_loop(0, nz, send_plane, 0)
     crecv[ep] = csend[c]
+
+    for t in range(rows):
+        key_columns = jnp.broadcast_to(akey[t : t + 1, :], (LANES, LANES)).T
+        key_columns = jnp.concatenate([key_columns] * (wv.shape[1] // LANES), axis=1)
+        state[t] = keep[t : t + 1, :] * mem[t] + key_columns * value[t : t + 1, :]
+    keeps.append(pltpu.make_async_copy(state, state_ref, out_sem.at[4]))
+    keeps[-1].start()
     others = crecv.at[pl.ds(0, chips * nc - 1)]
     plane = pltpu.make_async_remote_copy(
         src_ref=others,
@@ -461,7 +465,7 @@
     tgt_h,
     rw_h,
     pack_h,
-    mem_h,
+    state_h,
     mixed_ref,
     newmem_ref,
     newnorm_ref,
@@ -471,13 +475,12 @@
     tgt,
     rw,
     pack,
-    mem,
     state,
     load_sem,
-    mem_sem,
+    state_sem,
     sem,
 ):
-    rows, qk, dv = mem.shape
+    rows, qk, dv = state.shape
     chips, half, _ = parts.shape
     owned = 2 * half
     token_count = tgt.shape[1]
@@ -486,26 +489,21 @@
         ((pack_h, pack), (tgt_h, tgt), (parts_h, parts), (mid_h, mid), (rw_h, rw))
     ):
         loads.append(pltpu.make_async_copy(h, v, load_sem.at[i]))
-    mem_loads = [pltpu.make_async_copy(mem_h.at[t], mem.at[t], mem_sem.at[t]) for t in range(rows)]
-    for copy in loads + mem_loads:
+    moves = [pltpu.make_async_copy(state_h.at[t], state.at[t], state_sem.at[t]) for t in range(rows)]
+    for copy in loads + moves:
         copy.start()
     loads[0].wait()
+    newnorm_ref[...] = pack[:, 0:qk]
+    diagonal = lax.broadcasted_iota(jnp.int32, (rows, LANES), 0) == lax.broadcasted_iota(
+        jnp.int32, (rows, LANES), 1
+    )
+    newmax_ref[...] = jnp.sum(jnp.where(diagonal, pack[:, qk:], 0.0), axis=0, keepdims=True)[:, :rows]
     copies = []
-    value = pack[:, LANES + qk : LANES + qk + dv]
     for t in range(rows):
-        key_columns = jnp.broadcast_to(pack[t : t + 1, LANES : LANES + qk], (LANES, LANES)).T
-        key_columns = jnp.concatenate([key_columns] * (dv // LANES), axis=1)
-        mem_loads[t].wait()
-        state[t] = pack[t : t + 1, 0:1] * mem[t] + key_columns * value[t : t + 1, :]
+        moves[t].wait()
         copy = pltpu.make_async_copy(state.at[t], newmem_ref.at[t], sem.at[t])
         copy.start()
         copies.append(copy)
-    newnorm_ref[...] = pack[:, LANES + qk + dv : LANES + 2 * qk + dv]
-    diagonal = lax.broadcasted_iota(jnp.int32, (rows, LANES), 0) == lax.broadcasted_iota(
-        jnp.int32, (rows, LANES), 1
-    )
-    row = jnp.where(diagonal, pack[:, LANES + 2 * qk + dv :], 0.0)
-    newmax_ref[...] = jnp.sum(row, axis=0, keepdims=True)[:, :rows]
     for copy in loads[1:]:
         copy.wait()
 
@@ -601,17 +599,18 @@
     shape = jax.ShapeDtypeStruct
     vmem = pl.BlockSpec(memory_space=pltpu.VMEM)
     hbm = pl.BlockSpec(memory_space=pl.ANY)
-    pack_width = LANES * 2 + 2 * qk + dv
-    parts, mid, tgt, pack = pl.pallas_call(
+    pack_width = LANES + qk
+    parts, mid, tgt, pack, state = pl.pallas_call(
         functools.partial(kernel, sizes),
         out_shape=(
             shape((chips, owned // 2, LANES), BF16),
             shape((owned, token_count), BF16),
             shape((2, token_count), jnp.int32),
             shape((rows, pack_width), F32),
+            shape((rows, qk, dv), F32),
         ),
         in_specs=[hbm] * len(operands),
-        out_specs=(hbm,) * 4,
+        out_specs=(hbm,) * 5,
         scratch_shapes=[pltpu.VMEM(a.shape, a.dtype) for a in operands]
         + [
             pltpu.SemaphoreType.DMA((len(operands),)),
@@ -634,7 +633,9 @@
             pltpu.SemaphoreType.DMA((2, groups - 1)),
             pltpu.SemaphoreType.DMA((2,)),
             pltpu.SemaphoreType.DMA((2,)),
-            pltpu.SemaphoreType.DMA((4,)),
+            pltpu.SemaphoreType.DMA((5,)),
+            pltpu.SemaphoreType.REGULAR,
+            pltpu.VMEM((rows, qk, dv), F32),
         ],
         compiler_params=pltpu.CompilerParams(collective_id=0, has_side_effects=True),
     )(*operands)
@@ -655,12 +656,11 @@
             pltpu.VMEM((2, token_count), F32),
             pltpu.VMEM((rows, pack_width), F32),
             pltpu.VMEM((rows, qk, dv), F32),
-            pltpu.VMEM((rows, qk, dv), F32),
             pltpu.SemaphoreType.DMA((5,)),
             pltpu.SemaphoreType.DMA((rows,)),
             pltpu.SemaphoreType.DMA((rows,)),
         ],
-    )(parts, mid, tgt, route_weight.T, pack, memory.reshape(rows, qk, dv))
+    )(parts, mid, tgt, route_weight.T, pack, state)
     return (mixed.T, state[:, None], new_norm[:, None], new_max.T)
 
 

time: 50.4 us -> 47.6 us (0.944)
  Pallas kernels: 49.6 us -> 46.8 us
    pallas_call x1, Pallas kernels: 46.2 us -> 44 us  [shards(): pl.pallas_call(functools.partial(kernel, sizes), out_shape=(shape((chips,...]
    pallas_call x1, Pallas kernels: 3.38 us -> 2.8 us  [shards(): pl.pallas_call(combine, out_shape=(shape((owned, token_count), BF16), sha...]
where the time goes in v3:
time: 47.6 us; the launch traced here: 47.4 us
  Pallas kernels  46.8 us (98%)
  between operations  0.65 us (1%)
    pallas_call x1, Pallas kernels, shards(): pl.pallas_call(functools.partial(kernel, sizes), out_shape=(shape((chips,...  44 us
    pallas_call x1, Pallas kernels, shards(): pl.pallas_call(combine, out_shape=(shape((owned, token_count), BF16), sha...  2.8 us

profile of v3, /device:TPU:1, one launch (start us, length us, event | category | flops | bytes accessed | tf_op | source)
XLA Modules:
  0.0 47.4 jit_solution(14124278516775116513)
XLA Ops:
  0.6 44.0 %shard_map.219 = (bf16[64,4,128]{2,1,0:T(4,128)(2,1)}, bf16[8,1024]{1,0:T(8,128)(2,1)}, s32[2,1024]{1,0:T(2,128)}, f32[8,256]{1,0:T(8,128)}, f32[8,128,256]{2,1,0:T(8,128)}) custom-call(bf16[8,1024]{1,0:T(8,128)(2,1)} %tok_h.1, f32[1,1024]{1,0:T(1,128)} %bitcast.30, bf16[1024,128]{1,0:T(8,128)(2,1)} %wq_h.1, bf16[1024,128]{1,0:T(8,128)(2,1)} %wk_h.1, ...), custom_call_target="tpu_custom_call" | custom-call | tf_op jit(solution)/shard_map/pallas_call | solution.py:603
  44.6 2.8 %shard_map.220 = (bf16[8,1024]{1,0:T(8,128)(2,1)}, f32[8,128,256]{2,1,0:T(8,128)}, f32[8,128]{1,0:T(8,128)}, f32[1,8]{1,0:T(1,128)}) custom-call(bf16[64,4,128]{2,1,0:T(4,128)(2,1)} %get-tuple-element.13.parts_h, bf16[8,1024]{1,0:T(8,128)(2,1)} %get-tuple-element.14.mid_h, s32[2,1024]{1,0:T(2,128)} %get-tuple-element.15.tgt_h, f32[2,1024]{1,0:T(2,128)} %bitcast.29, ...), custom_call_target="tpu_custom_call" | custom-call | tf_op jit(solution)/shard_map/pallas_call | solution.py:642

commit v4 on v3

--- a/solution.py
+++ b/solution.py
@@ -100,6 +100,9 @@
     owned = width // (chips * nc)
     owners = LANES // owned
     group = x * nc + c
+    side = y % 2
+    first_y = y - side
+    half_lanes = LANES // 2
     expert_count = chips * nc
     token_count = route.shape[1]
 
@@ -125,28 +128,60 @@
         for dc in range(nc):
             if dx + dc > 0:
                 greet((z, y, lax.rem(c + dc, nc), lax.rem(x + dx, nx)))
+    for dx in range(1, nx):
+        for dc in range(nc):
+            greet((z, y + 1 - 2 * side, lax.rem(c + dc, nc), lax.rem(x + dx, nx)))
     source_group = ep // owners
     source_x, source_c = source_group // nc, source_group % nc
     from_self = source_group == group
 
-    hbm = (tok_h, mix_h, wq_h, wk_h, wv_h, wo_h, wi_h, wf_h, fb_h, hg_h, wout_h, mem_h, nrm_h, rmax_h)
-    hbm += (fg_h, route_h, wgate_h, wup_h, wdown_h)
-    vmem = (tok, mix, wq, wk, wv, wo, wi, wf, fb, hg, wout, mem, nrm, rmax)
-    vmem += (fg, route, wgate, wup, wdown)
-    loads = [pltpu.make_async_copy(h, v, load_sem.at[i]) for i, (h, v) in enumerate(zip(hbm, vmem))]
-    for load in loads:
-        load.start()
-
-    for i in range(14):
-        loads[i].wait()
+    pairs = {
+        "tok": (tok_h, tok),
+        "mix": (mix_h, mix),
+        "wq": (wq_h, wq),
+        "wk": (wk_h, wk),
+        "wv": (wv_h, wv),
+        "wo": (wo_h, wo),
+        "wi": (wi_h, wi),
+        "wf": (wf_h, wf),
+        "fb": (fb_h, fb),
+        "rmax": (rmax_h, rmax),
+        "nrm": (nrm_h, nrm),
+        "mem": (mem_h, mem),
+        "hg": (hg_h, hg),
+        "wout": (wout_h, wout),
+        "route": (route_h, route),
+        "fg": (fg_h, fg),
+        "wgate": (wgate_h, wgate),
+        "wup": (wup_h, wup),
+        "wdown": (wdown_h, wdown),
+    }
+    loads = {
+        n: pltpu.make_async_copy(h, v, load_sem.at[i]) for i, (n, (h, v)) in enumerate(pairs.items())
+    }
+    late = ("fg", "wgate", "wup", "wdown")
+    for n in loads:
+        if n not in late:
+            loads[n].start()
+
+    def ready(*names):
+        for n in names:
+            loads[n].wait()
+
+    ready("tok", "mix")
     tokens = tok[...].astype(F32)
     mean = jnp.mean(tokens * tokens, axis=1, keepdims=True)
     normed = (tokens * lax.rsqrt(mean + EPS) * mix[...]).astype(BF16)
+    ready("wq")
     query16 = dot(normed, wq[...]).astype(BF16)
     query = query16.astype(F32)
+    ready("wk")
     scaled_key = dot(normed, wk[...]).astype(BF16).astype(F32) * wq.shape[1] ** (-0.5)
+    ready("wv")
     value = dot(normed, wv[...]).astype(BF16).astype(F32)
+    ready("wo")
     ogate = dot(normed, wo[...]).astype(BF16).astype(F32)
+    ready("wi", "wf", "fb", "rmax", "nrm")
     floats = normed.astype(F32)
     head_row = lax.broadcasted_iota(jnp.int32, wi.shape, 0) == x
     in_row = jnp.sum(jnp.where(head_row, wi[...].astype(F32), 0.0), axis=0, keepdims=True)
@@ -171,6 +206,7 @@
     qk = wq.shape[1]
     pack[:, 0:qk] = norm_state
     pack[:, qk:] = jnp.broadcast_to(new_max, (rows, LANES))
+    ready("mem")
     row_of = lax.broadcasted_iota(jnp.int32, value.shape, 0)
     kept = jnp.zeros_like(value)
     for t in range(rows):
@@ -179,11 +215,12 @@
     denom = jnp.sum(query * norm_state, axis=1, keepdims=True)
     read = numer / jnp.maximum(jnp.abs(denom), jnp.exp(-new_max))
     scale = lax.rsqrt(jnp.mean(read * read, axis=1, keepdims=True) + EPS)
+    ready("hg", "wout")
     gated = (jax.nn.sigmoid(ogate) * read * scale * hg[...]).astype(BF16)
     partial = dot(gated, wout[...]).astype(BF16)
     for i in range(nx):
         psend[i] = partial[:, i * quarter : (i + 1) * quarter]
-    pl.semaphore_wait(barrier, (nz - 1) * nc + ny - 1 + nx * nc - 1)
+    pl.semaphore_wait(barrier, (nz - 1) * nc + ny - 1 + nx * nc - 1 + (nx - 1) * nc)
 
     for dy in y_order[:-1]:
         pl.semaphore_signal(
@@ -201,7 +238,9 @@
             device_id_type=MESH,
         ).start()
 
-    loads[15].wait()
+    for n in late:
+        loads[n].start()
+    ready("route")
     expert_of = lax.broadcasted_iota(jnp.int32, (expert_count, token_count), 0)
     named = [expert_of == route[j : j + 1, :] for j in range(2)]
     either = jnp.where(jnp.logical_or(named[0], named[1]), 1.0, 0.0)
@@ -221,7 +260,9 @@
         slot = jnp.sum(jnp.where(named[j], before, 0.0), axis=0, keepdims=True)
         tgt[j : j + 1, :] = route[j : j + 1, :] * CAP + slot.astype(jnp.int32)
     slots_here = nc * CAP
-    slot_id = lax.broadcasted_iota(jnp.int32, (slots_here, token_count), 0) + zy * slots_here
+    slots_both = 2 * slots_here
+    first_slot = (z * ny + first_y) * slots_here
+    slot_id = lax.broadcasted_iota(jnp.int32, (slots_both, token_count), 0) + first_slot
     hit = jnp.logical_or(slot_id == tgt[0:1, :], slot_id == tgt[1:2, :])
     place[...] = jnp.where(hit, 1.0, 0.0).astype(BF16)
     keeps = [
@@ -244,16 +285,21 @@
         copy.wait_recv()
         total = total + precv[dx - 1].astype(F32)
     own = tok[:, pl.ds(pl.multiple_of(x * quarter, quarter), quarter)].astype(F32)
-    middle = (own + total).astype(BF16)
+    middle = (own + total).astype(BF16).astype(F32)
+    token_half = rows // 2
+    low_rows = lax.broadcasted_iota(jnp.int32, (token_half, LANES), 1) < half_lanes
     for i in range(nc):
-        csend[i] = middle[:, i * LANES : (i + 1) * LANES]
+        tile = middle[:, i * LANES : (i + 1) * LANES]
+        turned = pltpu.roll(tile, half_lanes, 1)
+        csend[i, 0] = jnp.where(low_rows, tile[:token_half], turned[token_half:]).astype(BF16)
+        csend[i, 1] = jnp.where(low_rows, turned[:token_half], tile[token_half:]).astype(BF16)
 
     def send_plane(i, carry):
         tz = ring_z(i)
 
         def send(ty, tc):
             pltpu.make_async_remote_copy(
-                src_ref=csend.at[tc],
+                src_ref=csend.at[tc, ty % 2],
                 dst_ref=crecv.at[ep],
                 send_sem=csem.at[0],
                 recv_sem=csem.at[1],
@@ -276,7 +322,7 @@
 
     pl.semaphore_wait(plane_sem, ny - 1)
     lax.fori_loop(0, nz, send_plane, 0)
-    crecv[ep] = csend[c]
+    crecv[ep] = csend[c, side]
 
     for t in range(rows):
         key_columns = jnp.broadcast_to(akey[t : t + 1, :], (LANES, LANES)).T
@@ -294,15 +340,23 @@
         device_id_type=MESH,
     )
     plane.wait_recv()
-    everyone32 = crecv[...].astype(F32).reshape(token_count, LANES)
-    slots = dot(place[...], everyone32.astype(BF16)).astype(BF16)
-    for i in range(nc):
-        esend[i] = slots[i * CAP : (i + 1) * CAP]
+    packed = crecv[...].astype(F32)
+    everyone32 = jnp.concatenate([packed, pltpu.roll(packed, half_lanes, 2)], axis=1)
+    everyone32 = everyone32.reshape(token_count, LANES)
+    slots = dot(place[...], everyone32.astype(BF16))
+    half_cap = CAP // 2
+    low_slots = lax.broadcasted_iota(jnp.int32, (half_cap, LANES), 1) < half_lanes
+    for i in range(2 * nc):
+        upper = slots[i * CAP : i * CAP + half_cap]
+        lower = slots[i * CAP + half_cap : (i + 1) * CAP]
+        esend[i] = jnp.where(low_slots, upper, pltpu.roll(lower, half_lanes, 1)).astype(BF16)
+
+    x_order = sorted(range(nx), key=lambda d: -min(d, nx - d))
 
     def chip_row(send, recv, sem, src_of, dst):
         copies = []
-        for dx in range(nx):
-            for dc in range(nc):
+        for dx in x_order:
+            for dc in reversed(range(nc)):
                 if dx == 0 and dc == 0:
                     continue
                 tx, tc = lax.rem(x + dx, nx), lax.rem(c + dc, nc)
@@ -319,21 +373,46 @@
                 copies.append(copy)
         return copies
 
-    to_experts = chip_row(esend, erecv, esem, lambda tx, tc: tc, group)
-    erecv[group] = esend[c]
-
-    @pl.when(from_self)
+    to_experts = []
+    for dx in x_order:
+        for dy in (1, 0):
+            for dc in reversed(range(nc)):
+                if dx + dy + dc > 0:
+                    tx, tc = lax.rem(x + dx, nx), lax.rem(c + dc, nc)
+                    there = side if dy == 0 else 1 - side
+                    copy = pltpu.make_async_remote_copy(
+                        src_ref=esend.at[there * nc + tc],
+                        dst_ref=erecv.at[group, side],
+                        send_sem=esem.at[0, len(to_experts)],
+                        recv_sem=esem.at[1, len(to_experts)],
+                        device_id=(z, first_y + there, tc, tx),
+                        device_id_type=MESH,
+                    )
+                    copy.start()
+                    to_experts.append(copy)
+    erecv[group, side] = esend[side * nc + c]
+
+    serves = jnp.logical_and(from_self, y // (ny // 2) == side)
+    own_half = lax.rem(y, ny // 2) * nc + c
+
+    @pl.when(serves)
     def _():
         turned = everyone32.T
-        for k in range(owners):
+        for k in range(owners // 2):
             msend[k] = turned[k * owned : (k + 1) * owned, :].astype(BF16)
-        pltpu.make_async_copy(msend.at[lax.rem(ep, owners)], mrecv, out_sem.at[2]).start()
-
-    for i in (14, 16, 17, 18):
-        loads[i].wait()
+        pltpu.make_async_copy(msend.at[own_half], mrecv, out_sem.at[2]).start()
+
+    ready(*late)
     for copy in to_experts:
         copy.wait_recv()
-    stacked = jnp.concatenate([erecv[i] for i in range(groups)], axis=1).astype(F32)
+    stacked = []
+    for i in range(groups):
+        left, right = erecv[i, 0].astype(F32), erecv[i, 1].astype(F32)
+        left_turned = pltpu.roll(left, half_lanes, 1)
+        right_turned = pltpu.roll(right, half_lanes, 1)
+        tile = [jnp.where(low_slots, left, right_turned), jnp.where(low_slots, left_turned, right)]
+        stacked.append(jnp.concatenate(tile, axis=0))
+    stacked = jnp.concatenate(stacked, axis=1)
     mean = jnp.mean(stacked * stacked, axis=1, keepdims=True)
     routed = (stacked * lax.rsqrt(mean + EPS) * fg[...]).astype(BF16)
     gate_v = dot(routed, wgate[...])
@@ -347,21 +426,23 @@
     rrecv[group] = rsend[group]
 
     middle_copies = []
-    for dx in range(nx):
-        for dc in range(nc):
-            if dx + dc > 0:
-                tx, tc = lax.rem(x + dx, nx), lax.rem(c + dc, nc)
-                copy = pltpu.make_async_remote_copy(
-                    src_ref=msend.at[lax.rem(y * nc + tc, owners)],
-                    dst_ref=mrecv,
-                    send_sem=msem.at[0],
-                    recv_sem=msem.at[1],
-                    device_id=(z, y, tc, tx),
-                    device_id_type=MESH,
-                )
-                middle_copies.append(copy)
-
-    @pl.when(from_self)
+    for dx in x_order:
+        for dy in (1, 0):
+            for dc in reversed(range(nc)):
+                if dx + dy + dc > 0:
+                    tx, tc = lax.rem(x + dx, nx), lax.rem(c + dc, nc)
+                    ty = y if dy == 0 else y + 1 - 2 * side
+                    copy = pltpu.make_async_remote_copy(
+                        src_ref=msend.at[lax.rem(ty, ny // 2) * nc + tc],
+                        dst_ref=mrecv,
+                        send_sem=msem.at[0],
+                        recv_sem=msem.at[1],
+                        device_id=(z, ty, tc, tx),
+                        device_id_type=MESH,
+                    )
+                    middle_copies.append(copy)
+
+    @pl.when(serves)
     def _():
         for copy in middle_copies:
             copy.start()
@@ -393,7 +474,7 @@
                 device_id_type=MESH,
             ).start()
 
-        for dx in sorted(range(nx), key=lambda d: -min(d, nx - d)):
+        for dx in x_order:
             tx = lax.rem(x + dx, nx)
             for dc in reversed(range(nc)):
                 tc = lax.rem(c + dc, nc)
@@ -425,12 +506,18 @@
         own.start()
         arrivals(chips - 1).wait_recv()
         own.wait()
-        pltpu.make_async_copy(msend.at[lax.rem(ep, owners)], mrecv, out_sem.at[2]).wait()
 
     @pl.when(jnp.logical_not(from_self))
     def _():
+        arrivals(chips).wait_recv()
+
+    @pl.when(serves)
+    def _():
+        pltpu.make_async_copy(msend.at[own_half], mrecv, out_sem.at[2]).wait()
+
+    @pl.when(jnp.logical_not(serves))
+    def _():
         middle_copies[0].wait_recv()
-        arrivals(chips).wait_recv()
 
     for copy in keeps:
         copy.wait()
@@ -450,13 +537,16 @@
 
     @pl.when(from_self)
     def _():
+        arrivals(chips - 1).wait_send()
+
+    @pl.when(jnp.logical_not(from_self))
+    def _():
+        arrivals(chips).wait_send()
+
+    @pl.when(serves)
+    def _():
         for copy in middle_copies:
             copy.wait_send()
-        arrivals(chips - 1).wait_send()
-
-    @pl.when(jnp.logical_not(from_self))
-    def _():
-        arrivals(chips).wait_send()
 
 
 def combine(
@@ -616,20 +706,20 @@
             pltpu.SemaphoreType.DMA((len(operands),)),
             pltpu.VMEM((2, token_count), jnp.int32),
             pltpu.VMEM((rows, pack_width), F32),
-            pltpu.VMEM((nc * CAP, token_count), BF16),
+            pltpu.VMEM((2 * nc * CAP, token_count), BF16),
             pltpu.VMEM((nx, rows, quarter), BF16),
             pltpu.VMEM((nx - 1, rows, quarter), BF16),
-            pltpu.VMEM((nc, rows, LANES), BF16),
-            pltpu.VMEM((chips * nc, rows, LANES), BF16),
-            pltpu.VMEM((nc, CAP, LANES), BF16),
+            pltpu.VMEM((nc, 2, rows // 2, LANES), BF16),
+            pltpu.VMEM((chips * nc, rows // 2, LANES), BF16),
+            pltpu.VMEM((2 * nc, CAP // 2, LANES), BF16),
+            pltpu.VMEM((groups, 2, CAP // 2, LANES), BF16),
             pltpu.VMEM((groups, CAP, LANES), BF16),
             pltpu.VMEM((groups, CAP, LANES), BF16),
-            pltpu.VMEM((groups, CAP, LANES), BF16),
-            pltpu.VMEM((owners, owned, token_count), BF16),
+            pltpu.VMEM((owners // 2, owned, token_count), BF16),
             pltpu.VMEM((owners, owned // 2, LANES), BF16),
             pltpu.SemaphoreType.DMA((2, nx - 1)),
             pltpu.SemaphoreType.DMA((2,)),
-            pltpu.SemaphoreType.DMA((2, groups - 1)),
+            pltpu.SemaphoreType.DMA((2, 2 * groups - 1)),
             pltpu.SemaphoreType.DMA((2, groups - 1)),
             pltpu.SemaphoreType.DMA((2,)),
             pltpu.SemaphoreType.DMA((2,)),

time: 47.6 us -> 46.4 us (0.975)
  Pallas kernels: 46.8 us -> 45.6 us
    pallas_call x1, Pallas kernels: 44 us -> 42.8 us  [shards(): pl.pallas_call(functools.partial(kernel, sizes), out_shape=(shape((chips,...]
where the time goes in v4:
time: 46.4 us; the launch traced here: 46.2 us
  Pallas kernels  45.6 us (98%)
  between operations  0.65 us (1%)
    pallas_call x1, Pallas kernels, shards(): pl.pallas_call(functools.partial(kernel, sizes), out_shape=(shape((chips,...  42.8 us
    pallas_call x1, Pallas kernels, shards(): pl.pallas_call(combine, out_shape=(shape((owned, token_count), BF16), sha...  2.8 us

profile of v4, /device:TPU:1, one launch (start us, length us, event | category | flops | bytes accessed | tf_op | source)
XLA Modules:
  0.0 46.2 jit_solution(14431486273914373446)
XLA Ops:
  0.6 42.8 %shard_map.219 = (bf16[64,4,128]{2,1,0:T(4,128)(2,1)}, bf16[8,1024]{1,0:T(8,128)(2,1)}, s32[2,1024]{1,0:T(2,128)}, f32[8,256]{1,0:T(8,128)}, f32[8,128,256]{2,1,0:T(8,128)}) custom-call(bf16[8,1024]{1,0:T(8,128)(2,1)} %tok_h.1, f32[1,1024]{1,0:T(1,128)} %bitcast.30, bf16[1024,128]{1,0:T(8,128)(2,1)} %wq_h.1, bf16[1024,128]{1,0:T(8,128)(2,1)} %wk_h.1, ...), custom_call_target="tpu_custom_call" | custom-call | tf_op jit(solution)/shard_map/pallas_call | solution.py:693
  43.4 2.8 %shard_map.220 = (bf16[8,1024]{1,0:T(8,128)(2,1)}, f32[8,128,256]{2,1,0:T(8,128)}, f32[8,128]{1,0:T(8,128)}, f32[1,8]{1,0:T(1,128)}) custom-call(bf16[64,4,128]{2,1,0:T(4,128)(2,1)} %get-tuple-element.13.parts_h, bf16[8,1024]{1,0:T(8,128)(2,1)} %get-tuple-element.14.mid_h, s32[2,1024]{1,0:T(2,128)} %get-tuple-element.15.tgt_h, f32[2,1024]{1,0:T(2,128)} %bitcast.29, ...), custom_call_target="tpu_custom_call" | custom-call | tf_op jit(solution)/shard_map/pallas_call | solution.py:732

commit v5 on v4

--- a/solution.py
+++ b/solution.py
@@ -106,35 +106,6 @@
     expert_count = chips * nc
     token_count = route.shape[1]
 
-    barrier = pltpu.get_barrier_semaphore()
-
-    def greet(target):
-        pl.semaphore_signal(barrier, inc=1, device_id=target, device_id_type=MESH)
-
-    y_order = sorted(range(ny), key=lambda d: -min(d, ny - d))
-
-    def ring_z(i):
-        shift = nz // 2 + jnp.where(i % 2 == 0, i // 2, -((i + 1) // 2))
-        return lax.rem(z + shift, nz)
-
-    z_order = sorted(range(1, nz), key=lambda d: -min(d, nz - d))
-    for dz in z_order:
-        tz = lax.rem(z + dz, nz)
-        for dc in range(nc):
-            greet((tz, y, lax.rem(c + dc, nc), x))
-    for dy in y_order[:-1]:
-        greet((z, lax.rem(y + dy, ny), c, x))
-    for dx in range(nx):
-        for dc in range(nc):
-            if dx + dc > 0:
-                greet((z, y, lax.rem(c + dc, nc), lax.rem(x + dx, nx)))
-    for dx in range(1, nx):
-        for dc in range(nc):
-            greet((z, y + 1 - 2 * side, lax.rem(c + dc, nc), lax.rem(x + dx, nx)))
-    source_group = ep // owners
-    source_x, source_c = source_group // nc, source_group % nc
-    from_self = source_group == group
-
     pairs = {
         "tok": (tok_h, tok),
         "mix": (mix_h, mix),
@@ -168,6 +139,36 @@
         for n in names:
             loads[n].wait()
 
+    barrier = pltpu.get_barrier_semaphore()
+
+    def greet(target):
+        pl.semaphore_signal(barrier, inc=1, device_id=target, device_id_type=MESH)
+
+    y_order = sorted(range(ny), key=lambda d: -min(d, ny - d))
+
+    def ring_z(i):
+        shift = nz // 2 + jnp.where(i % 2 == 0, i // 2, -((i + 1) // 2))
+        return lax.rem(z + shift, nz)
+
+    z_order = sorted(range(1, nz), key=lambda d: -min(d, nz - d))
+    for dz in z_order:
+        tz = lax.rem(z + dz, nz)
+        for dc in range(nc):
+            greet((tz, y, lax.rem(c + dc, nc), x))
+    for dy in y_order[:-1]:
+        greet((z, lax.rem(y + dy, ny), c, x))
+    for dx in range(nx):
+        for dc in range(nc):
+            if dx + dc > 0:
+                greet((z, y, lax.rem(c + dc, nc), lax.rem(x + dx, nx)))
+    for dx in range(1, nx):
+        for dc in range(nc):
+            greet((z, y + 1 - 2 * side, lax.rem(c + dc, nc), lax.rem(x + dx, nx)))
+    source_group = ep // owners
+    from_self = source_group == group
+    result_group = lax.rem(x + nx - lax.rem(z, nx), nx) * nc + c
+    result_from_self = source_group == result_group
+
     ready("tok", "mix")
     tokens = tok[...].astype(F32)
     mean = jnp.mean(tokens * tokens, axis=1, keepdims=True)
@@ -177,9 +178,8 @@
     query = query16.astype(F32)
     ready("wk")
     scaled_key = dot(normed, wk[...]).astype(BF16).astype(F32) * wq.shape[1] ** (-0.5)
-    ready("wv")
+    ready("wv", "wo")
     value = dot(normed, wv[...]).astype(BF16).astype(F32)
-    ready("wo")
     ogate = dot(normed, wo[...]).astype(BF16).astype(F32)
     ready("wi", "wf", "fb", "rmax", "nrm")
     floats = normed.astype(F32)
@@ -206,7 +206,7 @@
     qk = wq.shape[1]
     pack[:, 0:qk] = norm_state
     pack[:, qk:] = jnp.broadcast_to(new_max, (rows, LANES))
-    ready("mem")
+    ready("mem", "hg", "wout")
     row_of = lax.broadcasted_iota(jnp.int32, value.shape, 0)
     kept = jnp.zeros_like(value)
     for t in range(rows):
@@ -215,7 +215,6 @@
     denom = jnp.sum(query * norm_state, axis=1, keepdims=True)
     read = numer / jnp.maximum(jnp.abs(denom), jnp.exp(-new_max))
     scale = lax.rsqrt(jnp.mean(read * read, axis=1, keepdims=True) + EPS)
-    ready("hg", "wout")
     gated = (jax.nn.sigmoid(ogate) * read * scale * hg[...]).astype(BF16)
     partial = dot(gated, wout[...]).astype(BF16)
     for i in range(nx):
@@ -227,7 +226,8 @@
             plane_sem, inc=1, device_id=(z, lax.rem(y + dy, ny), c, x), device_id_type=MESH
         )
 
-    for dx in range(1, nx):
+    x_order = sorted(range(nx), key=lambda d: -min(d, nx - d))
+    for dx in x_order[:-1]:
         tx = lax.rem(x + dx, nx)
         pltpu.make_async_remote_copy(
             src_ref=psend.at[tx],
@@ -351,8 +351,6 @@
         lower = slots[i * CAP + half_cap : (i + 1) * CAP]
         esend[i] = jnp.where(low_slots, upper, pltpu.roll(lower, half_lanes, 1)).astype(BF16)
 
-    x_order = sorted(range(nx), key=lambda d: -min(d, nx - d))
-
     def chip_row(send, recv, sem, src_of, dst):
         copies = []
         for dx in x_order:
@@ -422,8 +420,11 @@
     for i in range(groups):
         rsend[i] = down[:, i * LANES : (i + 1) * LANES]
 
-    to_groups = chip_row(rsend, rrecv, rsem, lambda tx, tc: tx * nc + tc, group)
-    rrecv[group] = rsend[group]
+    def result_of(tx, tc):
+        return lax.rem(tx + nx - lax.rem(z, nx), nx) * nc + tc
+
+    to_groups = chip_row(rsend, rrecv, rsem, result_of, group)
+    rrecv[group] = rsend[result_group]
 
     middle_copies = []
     for dx in x_order:
@@ -470,7 +471,7 @@
                 dst_ref=frecv.at[zy],
                 send_sem=dsem.at[0],
                 recv_sem=dsem.at[1],
-                device_id=(group, ty, tc, tx),
+                device_id=(result_group, ty, tc, tx),
                 device_id_type=MESH,
             ).start()
 
@@ -480,7 +481,7 @@
                 tc = lax.rem(c + dc, nc)
                 if dx == 0 and dc == 0:
 
-                    @pl.when(jnp.logical_not(jnp.logical_and(from_self, i == ny - 1)))
+                    @pl.when(jnp.logical_not(jnp.logical_and(result_from_self, i == ny - 1)))
                     def _():
                         send(tc, tx)
                 else:
@@ -500,14 +501,14 @@
             device_id_type=MESH,
         )
 
-    @pl.when(from_self)
+    @pl.when(result_from_self)
     def _():
         own = pltpu.make_async_copy(dsend.at[lax.rem(ep, owners)], frecv.at[zy], out_sem.at[3])
         own.start()
         arrivals(chips - 1).wait_recv()
         own.wait()
 
-    @pl.when(jnp.logical_not(from_self))
+    @pl.when(jnp.logical_not(result_from_self))
     def _():
         arrivals(chips).wait_recv()
 
@@ -535,11 +536,11 @@
     for copy in to_experts + to_groups:
         copy.wait_send()
 
-    @pl.when(from_self)
+    @pl.when(result_from_self)
     def _():
         arrivals(chips - 1).wait_send()
 
-    @pl.when(jnp.logical_not(from_self))
+    @pl.when(jnp.logical_not(result_from_self))
     def _():
         arrivals(chips).wait_send()
 
@@ -547,6 +548,10 @@
     def _():
         for copy in middle_copies:
             copy.wait_send()
+
+
+def lane_of(name):
+    return jnp.bitwise_and(name, LANES - 1).astype(F32).astype(BF16)
 
 
 def combine(
@@ -556,10 +561,13 @@
     rw_h,
     pack_h,
     state_h,
-    mixed_ref,
-    newmem_ref,
-    newnorm_ref,
-    newmax_ref,
+    mixed_h,
+    newmem_h,
+    newnorm_h,
+    newmax_h,
+    mixed,
+    newnorm,
+    newmax,
     parts,
     mid,
     tgt,
@@ -576,22 +584,22 @@
     token_count = tgt.shape[1]
     loads = []
     for i, (h, v) in enumerate(
-        ((pack_h, pack), (tgt_h, tgt), (parts_h, parts), (mid_h, mid), (rw_h, rw))
+        ((pack_h, pack), (parts_h, parts), (tgt_h, tgt), (mid_h, mid), (rw_h, rw))
     ):
         loads.append(pltpu.make_async_copy(h, v, load_sem.at[i]))
     moves = [pltpu.make_async_copy(state_h.at[t], state.at[t], state_sem.at[t]) for t in range(rows)]
     for copy in loads + moves:
         copy.start()
     loads[0].wait()
-    newnorm_ref[...] = pack[:, 0:qk]
+    newnorm[...] = pack[:, 0:qk]
     diagonal = lax.broadcasted_iota(jnp.int32, (rows, LANES), 0) == lax.broadcasted_iota(
         jnp.int32, (rows, LANES), 1
     )
-    newmax_ref[...] = jnp.sum(jnp.where(diagonal, pack[:, qk:], 0.0), axis=0, keepdims=True)[:, :rows]
+    newmax[...] = jnp.sum(jnp.where(diagonal, pack[:, qk:], 0.0), axis=0, keepdims=True)[:, :rows]
     copies = []
     for t in range(rows):
         moves[t].wait()
-        copy = pltpu.make_async_copy(state.at[t], newmem_ref.at[t], sem.at[t])
+        copy = pltpu.make_async_copy(state.at[t], newmem_h.at[t], sem.at[t])
         copy.start()
         copies.append(copy)
     for copy in loads[1:]:
@@ -606,13 +614,13 @@
         [jnp.where(low, even, odd_turned), jnp.where(low, even_turned, odd)], axis=1
     )
     held = held.reshape(chips // 2 * owned, LANES).astype(BF16)
-    lane_id = lax.broadcasted_iota(jnp.int32, (LANES, LANES), 0)
+    lane_id = lax.broadcasted_iota(jnp.int32, (LANES, LANES), 0).astype(F32).astype(BF16)
     for k in range(token_count // LANES):
         span = slice(k * LANES, (k + 1) * LANES)
         names = [tgt[j : j + 1, span] for j in range(2)]
         picks = jnp.concatenate(
             [
-                jnp.where(lane_id == jnp.bitwise_and(n, LANES - 1), 1.0, 0.0).astype(BF16)
+                jnp.where(lane_id == lane_of(n), jnp.ones((), BF16), jnp.zeros((), BF16))
                 for n in names
             ],
             axis=1,
@@ -628,7 +636,12 @@
             total.append(got)
         w0, w1 = rw[0:1, span], rw[1:2, span]
         weighed = total[0] * (w0 / (w0 + w1)) + total[1] * (w1 / (w0 + w1))
-        mixed_ref[:, span] = (mid[:, span].astype(F32) + weighed).astype(BF16)
+        mixed[:, span] = (mid[:, span].astype(F32) + weighed).astype(BF16)
+    outs = ((mixed, mixed_h), (newnorm, newnorm_h), (newmax, newmax_h))
+    for i, (v, h) in enumerate(outs):
+        copy = pltpu.make_async_copy(v, h, sem.at[rows + i])
+        copy.start()
+        copies.append(copy)
     for copy in copies:
         copy.wait()
 
@@ -687,7 +700,6 @@
         w_down[0],
     )
     shape = jax.ShapeDtypeStruct
-    vmem = pl.BlockSpec(memory_space=pltpu.VMEM)
     hbm = pl.BlockSpec(memory_space=pl.ANY)
     pack_width = LANES + qk
     parts, mid, tgt, pack, state = pl.pallas_call(
@@ -738,8 +750,11 @@
             shape((1, rows), F32),
         ),
         in_specs=[hbm] * 6,
-        out_specs=(vmem, hbm, vmem, vmem),
+        out_specs=(hbm,) * 4,
         scratch_shapes=[
+            pltpu.VMEM((owned, token_count), BF16),
+            pltpu.VMEM((rows, qk), F32),
+            pltpu.VMEM((1, rows), F32),
             pltpu.VMEM((chips, owned // 2, LANES), BF16),
             pltpu.VMEM((owned, token_count), BF16),
             pltpu.VMEM((2, token_count), jnp.int32),
@@ -748,7 +763,7 @@
             pltpu.VMEM((rows, qk, dv), F32),
             pltpu.SemaphoreType.DMA((5,)),
             pltpu.SemaphoreType.DMA((rows,)),
-            pltpu.SemaphoreType.DMA((rows,)),
+            pltpu.SemaphoreType.DMA((rows + 3,)),
         ],
     )(parts, mid, tgt, route_weight.T, pack, state)
     return (mixed.T, state[:, None], new_norm[:, None], new_max.T)

time: 46.4 us -> 46 us (level)
  no operation moved by 1% of the time
where the time goes in v5:
time: 46 us; the launch traced here: 45.8 us
  Pallas kernels  45.2 us (98%)
  between operations  0.65 us (1%)
    pallas_call x1, Pallas kernels, shards(): pl.pallas_call(functools.partial(kernel, sizes), out_shape=(shape((chips,...  42.5 us
    pallas_call x1, Pallas kernels, shards(): pl.pallas_call(combine, out_shape=(shape((owned, token_count), BF16), sha...  2.66 us

profile of v5, /device:TPU:1, one launch (start us, length us, event | category | flops | bytes accessed | tf_op | source)
XLA Modules:
  0.0 45.8 jit_solution(12798528897309307223)
XLA Ops:
  0.6 42.5 %shard_map.219 = (bf16[64,4,128]{2,1,0:T(4,128)(2,1)}, bf16[8,1024]{1,0:T(8,128)(2,1)}, s32[2,1024]{1,0:T(2,128)}, f32[8,256]{1,0:T(8,128)}, f32[8,128,256]{2,1,0:T(8,128)}) custom-call(bf16[8,1024]{1,0:T(8,128)(2,1)} %tok_h.1, f32[1,1024]{1,0:T(1,128)} %bitcast.30, bf16[1024,128]{1,0:T(8,128)(2,1)} %wq_h.1, bf16[1024,128]{1,0:T(8,128)(2,1)} %wk_h.1, ...), custom_call_target="tpu_custom_call" | custom-call | tf_op jit(solution)/shard_map/pallas_call | solution.py:705
  43.2 2.7 %shard_map.220 = (bf16[8,1024]{1,0:T(8,128)(2,1)}, f32[8,128,256]{2,1,0:T(8,128)}, f32[8,128]{1,0:T(8,128)}, f32[1,8]{1,0:T(1,128)}) custom-call(bf16[64,4,128]{2,1,0:T(4,128)(2,1)} %get-tuple-element.13.parts_h, bf16[8,1024]{1,0:T(8,128)(2,1)} %get-tuple-element.14.mid_h, s32[2,1024]{1,0:T(2,128)} %get-tuple-element.15.tgt_h, f32[2,1024]{1,0:T(2,128)} %bitcast.29, ...), custom_call_target="tpu_custom_call" | custom-call | tf_op jit(solution)/shard_map/pallas_call | solution.py:744

commit v6 on v5

--- a/solution.py
+++ b/solution.py
@@ -48,8 +48,7 @@
     state_ref,
     tok,
     mix,
-    wq,
-    wk,
+    wqk,
     wv,
     wo,
     wi,
@@ -62,8 +61,7 @@
     rmax,
     fg,
     route,
-    wgate,
-    wup,
+    wgateup,
     wdown,
     load_sem,
     tgt,
@@ -106,25 +104,27 @@
     expert_count = chips * nc
     token_count = route.shape[1]
 
+    qk = wqk.shape[1] // 2
+    hidden = wgateup.shape[1] // 2
     pairs = {
         "tok": (tok_h, tok),
         "mix": (mix_h, mix),
-        "wq": (wq_h, wq),
-        "wk": (wk_h, wk),
-        "wv": (wv_h, wv),
-        "wo": (wo_h, wo),
         "wi": (wi_h, wi),
         "wf": (wf_h, wf),
         "fb": (fb_h, fb),
         "rmax": (rmax_h, rmax),
         "nrm": (nrm_h, nrm),
+        "wq": (wq_h, wqk.at[:, 0:qk]),
+        "wk": (wk_h, wqk.at[:, qk : 2 * qk]),
+        "wv": (wv_h, wv),
+        "wo": (wo_h, wo),
         "mem": (mem_h, mem),
         "hg": (hg_h, hg),
         "wout": (wout_h, wout),
         "route": (route_h, route),
         "fg": (fg_h, fg),
-        "wgate": (wgate_h, wgate),
-        "wup": (wup_h, wup),
+        "wgate": (wgate_h, wgateup.at[:, 0:hidden]),
+        "wup": (wup_h, wgateup.at[:, hidden : 2 * hidden]),
         "wdown": (wdown_h, wdown),
     }
     loads = {
@@ -173,15 +173,11 @@
     tokens = tok[...].astype(F32)
     mean = jnp.mean(tokens * tokens, axis=1, keepdims=True)
     normed = (tokens * lax.rsqrt(mean + EPS) * mix[...]).astype(BF16)
-    ready("wq")
-    query16 = dot(normed, wq[...]).astype(BF16)
+    ready("wi", "wf", "fb", "rmax", "nrm", "wq", "wk")
+    query_key = dot(normed, wqk[...]).astype(BF16)
+    query16 = query_key[:, 0:qk]
     query = query16.astype(F32)
-    ready("wk")
-    scaled_key = dot(normed, wk[...]).astype(BF16).astype(F32) * wq.shape[1] ** (-0.5)
-    ready("wv", "wo")
-    value = dot(normed, wv[...]).astype(BF16).astype(F32)
-    ogate = dot(normed, wo[...]).astype(BF16).astype(F32)
-    ready("wi", "wf", "fb", "rmax", "nrm")
+    scaled_key = query_key[:, qk : 2 * qk].astype(F32) * qk ** (-0.5)
     floats = normed.astype(F32)
     head_row = lax.broadcasted_iota(jnp.int32, wi.shape, 0) == x
     in_row = jnp.sum(jnp.where(head_row, wi[...].astype(F32), 0.0), axis=0, keepdims=True)
@@ -203,10 +199,12 @@
     admit = jnp.exp(log_in - new_max)
     akey = admit * scaled_key
     norm_state = keep * nrm[...] + akey
-    qk = wq.shape[1]
     pack[:, 0:qk] = norm_state
     pack[:, qk:] = jnp.broadcast_to(new_max, (rows, LANES))
     ready("mem", "hg", "wout")
+    ready("wv", "wo")
+    value = dot(normed, wv[...]).astype(BF16).astype(F32)
+    ogate = dot(normed, wo[...]).astype(BF16).astype(F32)
     row_of = lax.broadcasted_iota(jnp.int32, value.shape, 0)
     kept = jnp.zeros_like(value)
     for t in range(rows):
@@ -411,10 +409,9 @@
         tile = [jnp.where(low_slots, left, right_turned), jnp.where(low_slots, left_turned, right)]
         stacked.append(jnp.concatenate(tile, axis=0))
     stacked = jnp.concatenate(stacked, axis=1)
-    mean = jnp.mean(stacked * stacked, axis=1, keepdims=True)
-    routed = (stacked * lax.rsqrt(mean + EPS) * fg[...]).astype(BF16)
-    gate_v = dot(routed, wgate[...])
-    up_v = dot(routed, wup[...])
+    scale = lax.rsqrt(jnp.mean(stacked * stacked, axis=1, keepdims=True) + EPS)
+    gate_up = dot((stacked * fg[...]).astype(BF16), wgateup[...]) * scale
+    gate_v, up_v = gate_up[:, 0:hidden], gate_up[:, hidden : 2 * hidden]
     act = (gate_v * jax.nn.sigmoid(gate_v) * up_v).astype(BF16)
     down = dot(act, wdown[...]).astype(BF16)
     for i in range(groups):
@@ -590,20 +587,14 @@
     moves = [pltpu.make_async_copy(state_h.at[t], state.at[t], state_sem.at[t]) for t in range(rows)]
     for copy in loads + moves:
         copy.start()
-    loads[0].wait()
+    for copy in loads:
+        copy.wait()
     newnorm[...] = pack[:, 0:qk]
     diagonal = lax.broadcasted_iota(jnp.int32, (rows, LANES), 0) == lax.broadcasted_iota(
         jnp.int32, (rows, LANES), 1
     )
     newmax[...] = jnp.sum(jnp.where(diagonal, pack[:, qk:], 0.0), axis=0, keepdims=True)[:, :rows]
     copies = []
-    for t in range(rows):
-        moves[t].wait()
-        copy = pltpu.make_async_copy(state.at[t], newmem_h.at[t], sem.at[t])
-        copy.start()
-        copies.append(copy)
-    for copy in loads[1:]:
-        copy.wait()
 
     low = lax.broadcasted_iota(jnp.int32, (chips // 2, half, LANES), 2) < LANES // 2
     both = parts[...].astype(F32).reshape(chips // 2, 2, half, LANES)
@@ -616,6 +607,12 @@
     held = held.reshape(chips // 2 * owned, LANES).astype(BF16)
     lane_id = lax.broadcasted_iota(jnp.int32, (LANES, LANES), 0).astype(F32).astype(BF16)
     for k in range(token_count // LANES):
+        if k == min(2, token_count // LANES - 1):
+            for t in range(rows):
+                moves[t].wait()
+                copy = pltpu.make_async_copy(state.at[t], newmem_h.at[t], sem.at[t])
+                copy.start()
+                copies.append(copy)
         span = slice(k * LANES, (k + 1) * LANES)
         names = [tgt[j : j + 1, span] for j in range(2)]
         picks = jnp.concatenate(
@@ -702,6 +699,10 @@
     shape = jax.ShapeDtypeStruct
     hbm = pl.BlockSpec(memory_space=pl.ANY)
     pack_width = LANES + qk
+    held = [pltpu.VMEM(a.shape, a.dtype) for a in operands]
+    held[2] = pltpu.VMEM((width, 2 * qk), BF16)
+    held[16] = pltpu.VMEM((width, 2 * w_gate.shape[2]), BF16)
+    del held[17], held[3]
     parts, mid, tgt, pack, state = pl.pallas_call(
         functools.partial(kernel, sizes),
         out_shape=(
@@ -713,7 +714,7 @@
         ),
         in_specs=[hbm] * len(operands),
         out_specs=(hbm,) * 5,
-        scratch_shapes=[pltpu.VMEM(a.shape, a.dtype) for a in operands]
+        scratch_shapes=held
         + [
             pltpu.SemaphoreType.DMA((len(operands),)),
             pltpu.VMEM((2, token_count), jnp.int32),

time: 46 us -> 45.9 us (level)
  no operation moved by 1% of the time
where the time goes in v6:
time: 45.9 us; the launch traced here: 45.7 us
  Pallas kernels  45.1 us (98%)
  between operations  0.65 us (1%)
    pallas_call x1, Pallas kernels, shards(): pl.pallas_call(functools.partial(kernel, sizes), out_shape=(shape((chips,...  42.5 us
    pallas_call x1, Pallas kernels, shards(): pl.pallas_call(combine, out_shape=(shape((owned, token_count), BF16), sha...  2.6 us

profile of v6, /device:TPU:1, one launch (start us, length us, event | category | flops | bytes accessed | tf_op | source)
XLA Modules:
  0.0 45.7 jit_solution(8263250920115514911)
XLA Ops:
  0.6 42.5 %shard_map.219 = (bf16[64,4,128]{2,1,0:T(4,128)(2,1)}, bf16[8,1024]{1,0:T(8,128)(2,1)}, s32[2,1024]{1,0:T(2,128)}, f32[8,256]{1,0:T(8,128)}, f32[8,128,256]{2,1,0:T(8,128)}) custom-call(bf16[8,1024]{1,0:T(8,128)(2,1)} %tok_h.1, f32[1,1024]{1,0:T(1,128)} %bitcast.30, bf16[1024,128]{1,0:T(8,128)(2,1)} %wq_h.1, bf16[1024,128]{1,0:T(8,128)(2,1)} %wk_h.1, ...), custom_call_target="tpu_custom_call" | custom-call | tf_op jit(solution)/shard_map/pallas_call | solution.py:706
  43.1 2.6 %shard_map.220 = (bf16[8,1024]{1,0:T(8,128)(2,1)}, f32[8,128,256]{2,1,0:T(8,128)}, f32[8,128]{1,0:T(8,128)}, f32[1,8]{1,0:T(1,128)}) custom-call(bf16[64,4,128]{2,1,0:T(4,128)(2,1)} %get-tuple-element.13.parts_h, bf16[8,1024]{1,0:T(8,128)(2,1)} %get-tuple-element.14.mid_h, s32[2,1024]{1,0:T(2,128)} %get-tuple-element.15.tgt_h, f32[2,1024]{1,0:T(2,128)} %bitcast.29, ...), custom_call_target="tpu_custom_call" | custom-call | tf_op jit(solution)/shard_map/pallas_call | solution.py:745

commit v7 on v6

--- a/solution.py
+++ b/solution.py
@@ -209,6 +209,12 @@
     kept = jnp.zeros_like(value)
     for t in range(rows):
         kept = jnp.where(row_of == t, dot(query16, mem[t].astype(BF16)), kept)
+    pl.semaphore_wait(barrier, (nz - 1) * nc + ny - 1 + nx * nc - 1 + (nx - 1) * nc)
+
+    for dy in y_order[:-1]:
+        pl.semaphore_signal(
+            plane_sem, inc=1, device_id=(z, lax.rem(y + dy, ny), c, x), device_id_type=MESH
+        )
     numer = keep * kept + jnp.sum(query * akey, axis=1, keepdims=True) * value
     denom = jnp.sum(query * norm_state, axis=1, keepdims=True)
     read = numer / jnp.maximum(jnp.abs(denom), jnp.exp(-new_max))
@@ -217,13 +223,6 @@
     partial = dot(gated, wout[...]).astype(BF16)
     for i in range(nx):
         psend[i] = partial[:, i * quarter : (i + 1) * quarter]
-    pl.semaphore_wait(barrier, (nz - 1) * nc + ny - 1 + nx * nc - 1 + (nx - 1) * nc)
-
-    for dy in y_order[:-1]:
-        pl.semaphore_signal(
-            plane_sem, inc=1, device_id=(z, lax.rem(y + dy, ny), c, x), device_id_type=MESH
-        )
-
     x_order = sorted(range(nx), key=lambda d: -min(d, nx - d))
     for dx in x_order[:-1]:
         tx = lax.rem(x + dx, nx)

time: 45.9 us -> 46.1 us (level)
  no operation moved by 1% of the time
where the time goes in v7:
time: 46.1 us; the launch traced here: 45.9 us
  Pallas kernels  45.3 us (98%)
  between operations  0.65 us (1%)
    pallas_call x1, Pallas kernels, shards(): pl.pallas_call(functools.partial(kernel, sizes), out_shape=(shape((chips,...  42.7 us
    pallas_call x1, Pallas kernels, shards(): pl.pallas_call(combine, out_shape=(shape((owned, token_count), BF16), sha...  2.6 us

profile of v7, /device:TPU:1, one launch (start us, length us, event | category | flops | bytes accessed | tf_op | source)
XLA Modules:
  0.0 45.9 jit_solution(5980836501360019786)
XLA Ops:
  0.6 42.7 %shard_map.219 = (bf16[64,4,128]{2,1,0:T(4,128)(2,1)}, bf16[8,1024]{1,0:T(8,128)(2,1)}, s32[2,1024]{1,0:T(2,128)}, f32[8,256]{1,0:T(8,128)}, f32[8,128,256]{2,1,0:T(8,128)}) custom-call(bf16[8,1024]{1,0:T(8,128)(2,1)} %tok_h.1, f32[1,1024]{1,0:T(1,128)} %bitcast.30, bf16[1024,128]{1,0:T(8,128)(2,1)} %wq_h.1, bf16[1024,128]{1,0:T(8,128)(2,1)} %wk_h.1, ...), custom_call_target="tpu_custom_call" | custom-call | tf_op jit(solution)/shard_map/pallas_call | solution.py:705
  43.3 2.6 %shard_map.220 = (bf16[8,1024]{1,0:T(8,128)(2,1)}, f32[8,128,256]{2,1,0:T(8,128)}, f32[8,128]{1,0:T(8,128)}, f32[1,8]{1,0:T(1,128)}) custom-call(bf16[64,4,128]{2,1,0:T(4,128)(2,1)} %get-tuple-element.13.parts_h, bf16[8,1024]{1,0:T(8,128)(2,1)} %get-tuple-element.14.mid_h, s32[2,1024]{1,0:T(2,128)} %get-tuple-element.15.tgt_h, f32[2,1024]{1,0:T(2,128)} %bitcast.29, ...), custom_call_target="tpu_custom_call" | custom-call | tf_op jit(solution)/shard_map/pallas_call | solution.py:744
